TPU v7x, 32 devices: a whole 2x2x4 slice. The times are simulated.
32 devices in a mesh: sp: 8 (over z, y), tp: 4 (over x, core).
Axes of the slice: x: 2, y: 2, z: 4, core: 2. Of those that a mesh axis runs over, the one named last changes fastest.
Arguments:
- activity: bfloat16 [2048, 4096], P('sp', 'tp'), may hold values from -8 to 8
- query_weight: bfloat16 [4096, 3072], P('sp', 'tp'), may hold values from -0.09375 to 0.09375
- key_weight: bfloat16 [4096, 3072], P('sp', 'tp'), may hold values from -0.09375 to 0.09375
- value_weight: bfloat16 [4096, 3072], P('sp', 'tp'), may hold values from -0.09375 to 0.09375
- merge_weight: bfloat16 [1024, 4096], P('tp', 'sp'), may hold values from -1.5 to 1.5
Outputs:
- attended: bfloat16 [2048, 4096], P(('sp', 'tp'))
All inputs are finite; a program needn't handle non-finite values.
Results may differ from a plain program's by a relative error of at most 0.013.
Values may be sent and summed in bfloat16 or wider, within the bound.
A program may use at most 128 MiB of HBM per device.

v0:
```python
import functools

import jax
import jax.numpy as jnp
from jax import lax
from jax.experimental import pallas as pl
from jax.experimental.pallas import tpu as pltpu
from jax.sharding import PartitionSpec as P

HEAD = 64
HEAD_GROUPS = 3
SPAN = 128
DILATIONS = (1, 4, 8)
MESH = pl.DeviceIdType.MESH

rope_base = 500000.0


def project_kernel(
    G, R, act, wq, wk, wv, cos_ref, sin_ref, out,
    a_buf, w_buf, c_buf, r_buf, q_buf, kv_buf, o_buf, m_buf,
    local_sem, swap_send, swap_recv, fan_send, fan_recv,
    w_send, w_recv, c_send, c_recv, kv_send, kv_recv, m_send, m_recv,
):
    s = lax.axis_index("sp")
    t = lax.axis_index("tp")
    g = lax.div(s, R)
    r = lax.rem(s, R)
    tok = act.shape[0]
    krows = wq.shape[0]
    width = wq.shape[1] // G
    pairs = G // 2
    weights = (wq, wk, wv)

    swap_dev = (t * R + r, g)
    barrier = pltpu.get_barrier_semaphore()

    def greet(dev):
        pl.semaphore_signal(barrier, inc=1, device_id=dev, device_id_type=MESH)

    for i in range(1, G):
        greet((s, lax.rem(t + i, G)))
        greet((lax.rem(g + i, G) * R + r, t))
    for i in range(1, R):
        greet((g * R + lax.rem(r + i, R), t))

    @pl.when(g != t)
    def _():
        greet(swap_dev)

    pl.semaphore_wait(barrier, 2 * (G - 1) + (R - 1) + jnp.where(g != t, 1, 0))

    def swap_copy():
        return pltpu.make_async_remote_copy(
            src_ref=act, dst_ref=a_buf.at[g], send_sem=swap_send, recv_sem=swap_recv,
            device_id=swap_dev, device_id_type=MESH)

    def swap_local():
        return pltpu.make_async_copy(act, a_buf.at[t], local_sem)

    @pl.when(g != t)
    def _():
        swap_copy().start()

    @pl.when(g == t)
    def _():
        swap_local().start()

    def pair_at(stage):
        return lax.rem(lax.div(g, 2) + 1 + stage, pairs)

    def pair_cols(stage):
        return pl.ds(pl.multiple_of(pair_at(stage) * (2 * width), 128), 2 * width)

    def w_copy(stage, i, x):
        cols = pair_cols(stage)
        return pltpu.make_async_remote_copy(
            src_ref=weights[x].at[:, cols], dst_ref=w_buf.at[i - 1, x, :, cols],
            send_sem=w_send.at[stage, i - 1, x], recv_sem=w_recv.at[stage, i - 1, x],
            device_id=(g * R + lax.rem(r + R - i, R), t), device_id_type=MESH)

    for stage in range(pairs):
        for i in range(1, R):
            for x in range(3):
                w_copy(stage, i, x).start()

    @pl.when(g != t)
    def _():
        swap_copy().wait_recv()

    @pl.when(g == t)
    def _():
        swap_local().wait()

    def fan_copy(i):
        return pltpu.make_async_remote_copy(
            src_ref=a_buf.at[t], dst_ref=a_buf.at[t], send_sem=fan_send.at[i - 1],
            recv_sem=fan_recv.at[i - 1],
            device_id=(s, lax.rem(t + i, G)), device_id_type=MESH)

    def fan_arrival(i):
        slot = lax.rem(t + G - i, G)
        return pltpu.make_async_remote_copy(
            src_ref=a_buf.at[slot], dst_ref=a_buf.at[slot], send_sem=fan_send.at[i - 1],
            recv_sem=fan_recv.at[i - 1],
            device_id=(s, lax.rem(t + i, G)), device_id_type=MESH)

    for i in range(1, G):
        fan_copy(i).start()
    for i in range(1, G):
        fan_arrival(i).wait_recv()

    def c_copy(stage, j, b):
        dest = pair_at(stage) * 2 + j
        rows = pl.ds(pl.multiple_of(b * tok, tok), tok)
        return pltpu.make_async_remote_copy(
            src_ref=c_buf.at[stage, j, rows], dst_ref=r_buf.at[g, rows],
            send_sem=c_send.at[stage, j, b], recv_sem=c_recv.at[g, b],
            device_id=(dest * R + r, t), device_id_type=MESH)

    for stage in range(pairs):
        for i in range(1, R):
            for x in range(3):
                w_copy(stage, i, x).wait_recv()
        cols = pair_cols(stage)

        @pl.loop(0, G)
        def _(b):
            parts = []
            for x in range(3):
                total = jnp.dot(
                    a_buf[b, :, pl.ds(pl.multiple_of(r * krows, 128), krows)],
                    weights[x][:, cols], preferred_element_type=jnp.float32)
                for i in range(1, R):
                    start = pl.multiple_of(lax.rem(r + i, R) * krows, 128)
                    total = total + jnp.dot(
                        a_buf[b, :, pl.ds(start, krows)], w_buf[i - 1, x, :, cols],
                        preferred_element_type=jnp.float32)
                parts.append(total)
            rows = pl.ds(pl.multiple_of(b * tok, tok), tok)
            for j in range(2):
                c_buf[stage, j, rows, :] = jnp.concatenate(
                    [part[:, j * width:(j + 1) * width] for part in parts], axis=1
                ).astype(jnp.bfloat16)
            for j in range(2):
                @pl.when(pair_at(stage) * 2 + j != g)
                def _():
                    c_copy(stage, j, b).start()

    def c_arrival(source, b):
        rows = pl.ds(pl.multiple_of(b * tok, tok), tok)
        return pltpu.make_async_remote_copy(
            src_ref=r_buf.at[source, rows], dst_ref=r_buf.at[source, rows],
            send_sem=c_send.at[0, 0, b], recv_sem=c_recv.at[source, b],
            device_id=(s, t), device_id_type=MESH)

    mine = lax.rem(g, 2)
    most = SPAN * DILATIONS[-1]
    kv_buf[0:most, :] = jnp.zeros((most, 2 * width), jnp.bfloat16)

    def kv_rows(b, part):
        return pl.ds(pl.multiple_of(most + (b * R + part) * tok, 128), tok)

    def kv_copy(i, b):
        rows = kv_rows(b, r)
        return pltpu.make_async_remote_copy(
            src_ref=kv_buf.at[rows], dst_ref=kv_buf.at[rows],
            send_sem=kv_send.at[i - 1, b], recv_sem=kv_recv.at[i - 1, b],
            device_id=(g * R + lax.rem(r + R - i, R), t), device_id_type=MESH)

    def kv_arrival(i, b):
        rows = kv_rows(b, lax.rem(r + i, R))
        return pltpu.make_async_remote_copy(
            src_ref=kv_buf.at[rows], dst_ref=kv_buf.at[rows],
            send_sem=kv_send.at[i - 1, b], recv_sem=kv_recv.at[i - 1, b],
            device_id=(g * R + lax.rem(r + R - i, R), t), device_id_type=MESH)

    def gather_block(b):
        rows = pl.ds(pl.multiple_of(b * tok, tok), tok)
        total = c_buf[pairs - 1, mine, rows, :].astype(jnp.float32)
        for i in range(1, G):
            source = lax.rem(g + i, G)
            c_arrival(source, b).wait_recv()
            total = total + r_buf[source, rows, :].astype(jnp.float32)
        turn = total[:, :2 * width]
        half = HEAD // 2
        ahead = jnp.concatenate([turn[:, half:], turn[:, :half]], axis=1)
        behind = jnp.concatenate([turn[:, -half:], turn[:, :-half]], axis=1)
        lane = lax.broadcasted_iota(jnp.int32, turn.shape, 1)
        other = jnp.where((lane & (HEAD - 1)) < half, ahead, behind)
        reps = 2 * width // cos_ref.shape[1]
        cosine = jnp.concatenate([cos_ref[rows, :]] * reps, axis=1)
        sine = jnp.concatenate([sin_ref[rows, :]] * reps, axis=1)
        turned = turn * cosine + other * sine
        q_buf[rows, :] = turned[:, :width].astype(jnp.bfloat16)
        kv_buf[kv_rows(b, r), :] = jnp.concatenate(
            [turned[:, width:], total[:, 2 * width:]], axis=1).astype(jnp.bfloat16)
        for i in range(1, R):
            kv_copy(i, b).start()

    def m_copy(b):
        return pltpu.make_async_remote_copy(
            src_ref=o_buf.at[b], dst_ref=m_buf.at[g],
            send_sem=m_send.at[b], recv_sem=m_recv.at[g],
            device_id=(b * R + r, t), device_id_type=MESH)

    def m_arrival(source):
        return pltpu.make_async_remote_copy(
            src_ref=m_buf.at[source], dst_ref=m_buf.at[source],
            send_sem=m_send.at[source], recv_sem=m_recv.at[source],
            device_id=(source * R + r, t), device_id_type=MESH)

    def attend(b):
        for i in range(1, R):
            kv_arrival(i, b).wait_recv()
        rows = pl.ds(pl.multiple_of(b * tok, tok), tok)
        first = (b * R + r) * tok
        mixed_list = []
        total_list = []
        for index, dilation in enumerate(DILATIONS):
            reach = SPAN * dilation
            keys = reach + tok
            near = pl.ds(pl.multiple_of(most - reach + first, 128), keys)
            q = q_buf[rows, index * HEAD:(index + 1) * HEAD]
            k = kv_buf[near, index * HEAD:(index + 1) * HEAD]
            v = kv_buf[near, width + index * HEAD:width + (index + 1) * HEAD]
            scores = lax.dot_general(
                q, k, (((1,), (1,)), ((), ())), preferred_element_type=jnp.float32
            ) * HEAD ** (-0.5)
            col = lax.broadcasted_iota(jnp.int32, (tok, keys), 1)
            gap = reach + lax.broadcasted_iota(jnp.int32, (tok, keys), 0) - col
            allowed = (gap >= 0) & (gap <= reach) & (col >= reach - first)
            if dilation > 1:
                allowed = allowed & ((gap & (dilation - 1)) == 0)
            scores = jnp.where(allowed, scores, -jnp.inf)
            row_max = jnp.max(scores, axis=1, keepdims=True)
            expo = jnp.exp(scores - row_max)
            denominator = jnp.sum(expo, axis=1, keepdims=True)
            mixed = jnp.dot(expo.astype(jnp.bfloat16), v, preferred_element_type=jnp.float32)
            mixed_list.append(mixed / denominator)
            total_list.append(row_max + jnp.log(denominator))
        peak = jnp.maximum(jnp.maximum(total_list[0], total_list[1]), total_list[2])
        shifted = [jnp.exp(one - peak) for one in total_list]
        whole = shifted[0] + shifted[1] + shifted[2]
        merged = sum(a / whole * b_ for a, b_ in zip(shifted, mixed_list)).astype(jnp.bfloat16)

        @pl.when(b != g)
        def _():
            o_buf[b] = merged
            m_copy(b).start()

        @pl.when(b == g)
        def _():
            m_buf[b] = merged

    gather_block(0)

    @pl.loop(1, G)
    def _(b):
        gather_block(b)
        attend(b - 1)

    attend(G - 1)

    for i in range(1, G):
        m_arrival(lax.rem(g + i, G)).wait_recv()
    out[...] = jnp.concatenate(
        [m_buf[h].astype(jnp.float32) for h in range(G)], axis=1).astype(jnp.bfloat16)

    for i in range(1, G):
        m_copy(lax.rem(g + i, G)).wait_send()

    @pl.loop(0, G)
    def _(b):
        for i in range(1, R):
            kv_copy(i, b).wait_send()

    @pl.when(g != t)
    def _():
        swap_copy().wait_send()

    for i in range(1, G):
        fan_copy(i).wait_send()
    for stage in range(pairs):
        for i in range(1, R):
            for x in range(3):
                w_copy(stage, i, x).wait_send()
        for j in range(2):
            @pl.when(pair_at(stage) * 2 + j != g)
            def _():
                @pl.loop(0, G)
                def _(b):
                    c_copy(stage, j, b).wait_send()


def project(activity, wq, wk, wv, cosine, sine, G, R):
    tok, feat = activity.shape
    krows, col_width = wq.shape
    width = 3 * (col_width // G)
    pairs = G // 2
    rows = G * tok
    dma = pltpu.SemaphoreType.DMA
    return pl.pallas_call(
        functools.partial(project_kernel, G, R),
        out_shape=jax.ShapeDtypeStruct((tok, G * HEAD), jnp.bfloat16),
        in_specs=[pl.BlockSpec(memory_space=pltpu.VMEM)] * 6,
        out_specs=pl.BlockSpec(memory_space=pltpu.VMEM),
        scratch_shapes=[
            pltpu.VMEM((G, tok, feat), jnp.bfloat16),
            pltpu.VMEM((R - 1, 3, krows, col_width), jnp.bfloat16),
            pltpu.VMEM((pairs, 2, rows, width), jnp.bfloat16),
            pltpu.VMEM((G, rows, width), jnp.bfloat16),
            pltpu.VMEM((rows, width // 3), jnp.bfloat16),
            pltpu.VMEM((SPAN * DILATIONS[-1] + R * rows, 2 * (width // 3)), jnp.bfloat16),
            pltpu.VMEM((G, tok, HEAD), jnp.bfloat16),
            pltpu.VMEM((G, tok, HEAD), jnp.bfloat16),
            dma, dma, dma, dma((G - 1,)), dma((G - 1,)),
            dma((pairs, R - 1, 3)), dma((pairs, R - 1, 3)),
            dma((pairs, 2, G)), dma((G, G)),
            dma((R - 1, G)), dma((R - 1, G)), dma((G,)), dma((G,)),
        ],
        compiler_params=pltpu.CompilerParams(
            collective_id=0, has_side_effects=True, vmem_limit_bytes=58 * 2**20),
        cost_estimate=pl.CostEstimate(
            flops=2 * rows * feat * 3 * col_width, bytes_accessed=300 * 2**20, transcendentals=0),
    )(activity, wq, wk, wv, cosine, sine)


def finish_kernel(merged, weight, out, near_out, near_in, far_out, far_in, held,
                  near_send, near_recv, far_send, far_recv):
    s = lax.axis_index("sp")
    t = lax.axis_index("tp")
    chunks = near_out.shape[0]
    rows = out.shape[0]
    cols = weight.shape[1] // chunks
    low = lax.rem(t, 2)
    near = t + 1 - 2 * low
    far = lax.rem(t + 2, 4)
    across = lax.rem(near + 2, 4)

    barrier = pltpu.get_barrier_semaphore()
    for peer in (near, far):
        pl.semaphore_signal(barrier, inc=1, device_id=(s, peer), device_id_type=MESH)
    pl.semaphore_wait(barrier, 2)

    def near_copy(c):
        return pltpu.make_async_remote_copy(
            src_ref=near_out.at[c], dst_ref=near_in.at[c], send_sem=near_send.at[c],
            recv_sem=near_recv.at[c], device_id=(s, near), device_id_type=MESH)

    def far_copy(c):
        return pltpu.make_async_remote_copy(
            src_ref=far_out.at[c], dst_ref=far_in.at[c], send_sem=far_send.at[c],
            recv_sem=far_recv.at[c], device_id=(s, far), device_id_type=MESH)

    def part(owner, at):
        picked = merged[pl.ds(pl.multiple_of(owner * rows, rows), rows), :]
        return jnp.dot(picked, weight[:, at], preferred_element_type=jnp.float32)

    @pl.loop(0, chunks)
    def _(c):
        at = pl.ds(pl.multiple_of(c * cols, 128), cols)
        near_out[c, 0] = part(across, at).astype(jnp.bfloat16)
        near_out[c, 1] = part(near, at).astype(jnp.bfloat16)
        near_copy(c).start()
        held[c, 0] = part(far, at)
        held[c, 1] = part(t, at)

    @pl.loop(0, chunks)
    def _(c):
        near_copy(c).wait_recv()
        far_out[c] = (held[c, 0] + near_in[c, 0].astype(jnp.float32)).astype(jnp.bfloat16)
        far_copy(c).start()
        held[c, 1] = held[c, 1] + near_in[c, 1].astype(jnp.float32)

    @pl.loop(0, chunks)
    def _(c):
        at = pl.ds(pl.multiple_of(c * cols, 128), cols)
        far_copy(c).wait_recv()
        out[:, at] = (held[c, 1] + far_in[c].astype(jnp.float32)).astype(jnp.bfloat16)

    @pl.loop(0, chunks)
    def _(c):
        near_copy(c).wait_send()
        far_copy(c).wait_send()


def finish(merged, weight, chunks):
    rows = merged.shape[0] // 4
    cols = weight.shape[1] // chunks
    dma = pltpu.SemaphoreType.DMA
    return pl.pallas_call(
        finish_kernel,
        out_shape=jax.ShapeDtypeStruct((rows, weight.shape[1]), jnp.bfloat16),
        in_specs=[pl.BlockSpec(memory_space=pltpu.VMEM)] * 2,
        out_specs=pl.BlockSpec(memory_space=pltpu.VMEM),
        scratch_shapes=[
            pltpu.VMEM((chunks, 2, rows, cols), jnp.bfloat16),
            pltpu.VMEM((chunks, 2, rows, cols), jnp.bfloat16),
            pltpu.VMEM((chunks, rows, cols), jnp.bfloat16),
            pltpu.VMEM((chunks, rows, cols), jnp.bfloat16),
            pltpu.VMEM((chunks, 2, rows, cols), jnp.float32),
            dma((chunks,)), dma((chunks,)), dma((chunks,)), dma((chunks,)),
        ],
        compiler_params=pltpu.CompilerParams(
            collective_id=1, has_side_effects=True, vmem_limit_bytes=40 * 2**20),
    )(merged, weight)


def per_device(activity, query_weight, key_weight, value_weight, merge_weight):
    G = lax.axis_size("tp")
    R = lax.axis_size("sp") // G
    r = lax.axis_index("sp") % R
    tok = activity.shape[0]
    merge_full = lax.all_gather(merge_weight, "sp", axis=1, tiled=True)
    block_start = (jnp.arange(G, dtype=jnp.int32) * R + r) * tok
    pos = (block_start[:, None] + jnp.arange(tok, dtype=jnp.int32)[None, :]).reshape(G * tok)
    half = HEAD // 2
    frequency = rope_base ** (-jnp.arange(0, half, dtype=jnp.float32) * 2.0 / HEAD)
    angles = pos.astype(jnp.float32)[:, None] * frequency[None, :]
    cosine = jnp.tile(jnp.cos(angles), (1, 4))
    sine = jnp.sin(angles)
    sine = jnp.tile(jnp.concatenate([-sine, sine], axis=1), (1, 2))
    merged = project(activity, query_weight, key_weight, value_weight, cosine, sine, G, R)
    return finish(merged, merge_full, 8)


def solution(mesh):
    placed = (P("sp", "tp"), P("sp", "tp"), P("sp", "tp"), P("sp", "tp"), P("tp", "sp"))
    return jax.shard_map(
        per_device, mesh=mesh, in_specs=placed, out_specs=P(("sp", "tp"), None), check_vma=False
    )
```

profile of v0, /device:TPU:25, one launch (start us, length us, event | category | flops | bytes accessed | tf_op | source)
XLA Modules:
  0.0 224.5 jit_solution(12454757120080427047)
XLA Ops:
  6.5 0.0 all-gather.2.cloned.1.call-start
  6.5 0.7 all-gather.2.cloned.1.call-update
  7.3 0.1 convert_bitcast_fusion
  7.4 0.5 fusion
  8.0 1.0 copy.7.sin_ref
  9.0 1.0 copy.6.cos_ref
  10.0 184.5 %shard_map.55.merged = bf16[256,256]{1,0:T(8,128)(2,1)} custom-call(bf16[256,1024]{1,0:T(8,128)(2,1)} %act.1, bf16[512,768]{1,0:T(8,128)(2,1)} %wq.1, bf16[512,768]{1,0:T(8,128)(2,1)} %wk.1, bf16[512,768]{1,0:T(8,128)(2,1)} %wv.1, f32[1024,128]{1,0:T(8,128)} %copy.6.cos_ref, f32[1024,128]{1,0:T(8,128)} %copy.7.sin_ref), custom_call_target="tpu_custom_call" | custom-call | flops 4831838208 | bytes 314572800 | tf_op jit(solution)/shard_map/pallas_call | solution.py:303
  194.6 0.0 all-gather.2.cloned.1.call-done.weight
  194.6 0.0 copy-start
  194.6 1.6 copy-done
  196.2 0.0 copy-start.1
  196.2 0.9 copy-done.1
  197.1 19.8 %shard_map.56 = bf16[64,4096]{1,0:T(8,128)(2,1)S(1)} custom-call(bf16[256,256]{1,0:T(8,128)(2,1)S(1)} %copy-done.1, bf16[256,4096]{1,0:T(8,128)(2,1)S(1)} %copy-done), custom_call_target="tpu_custom_call" | custom-call | tf_op jit(solution)/shard_map/pallas_call | solution.py:392
  216.9 0.8 copy.10
  (6 shorter events, 0.1 us)
Async XLA Ops:
  6.5 188.1 %all-gather.2.cloned.1.call-start = ((), (), s32[]{:S(2)}) async-start(), calls=%async_computation | async-start | bytes 2359296 | tf_op jit(solution)/shard_map/all_gather | solution.py:415
  194.6 1.6 copy-start
  196.2 0.9 copy-start.1
Sparse Core Ops, SparseCore 0:
  9.4 119.3 all-gather.1
where the time goes:
time: 225 us
  Pallas kernels  204 us (91%)
  between operations  13.5 us (6%)
  local copies, waits for them, and re-layouts  5.36 us (2%)
    pallas_call x1, Pallas kernels, project(): pl.pallas_call(functools.partial(project_kernel, G, R), out_shape=jax.Sha...  185 us
    pallas_call x1, Pallas kernels, finish(): pl.pallas_call(finish_kernel, out_shape=jax.ShapeDtypeStruct((rows, weigh...  19.8 us
  transfers between devices with their start and end apart: 1, of which 0 were waited for; matrix products, arithmetic and copies ran while one was open for 1% of the time, Pallas kernels for 82%

commit v1 on v0

--- a/solution.py
+++ b/solution.py
@@ -1,4 +1,5 @@
 import functools
+import math
 
 import jax
 import jax.numpy as jnp
@@ -407,12 +408,409 @@
     )(merged, weight)
 
 
+def halves_kernel(
+    act, wq, wk, wv, out,
+    x_buf, w_buf, own_buf, c_buf, r_buf, q_buf, kv_buf, o_buf, m_buf, cos_buf, sin_buf,
+    local_sem, w_local, x_send, x_recv, w_send, w_recv, c_send, c_recv,
+    kv_send, kv_recv, m_send, m_recv,
+):
+    s = lax.axis_index("sp")
+    t = lax.axis_index("tp")
+    z = lax.div(s, 2)
+    y = lax.rem(s, 2)
+    x = lax.div(t, 2)
+    c = lax.rem(t, 2)
+    zh = lax.div(z, 2)
+    zl = lax.rem(z, 2)
+    G = 4
+    tok, feat = act.shape
+    krows = wq.shape[0]
+    pair = wq.shape[1] // 2
+    width = pair // 2
+    part = tok // 2
+    weights = (wq, wk, wv)
+    z_near = z + 1 - 2 * zl
+    z_pair = lax.rem(z + 2, 4)
+    y_far = 1 - y
+    t_flip = 3 - t
+    t_core = t + 1 - 2 * c
+    hub = c == zh
+    inner = zl != zh
+    straight = c == x
+
+    def at_z(other):
+        return (other * 2 + y, t)
+
+    barrier = pltpu.get_barrier_semaphore()
+
+    def greet(dev):
+        pl.semaphore_signal(barrier, inc=1, device_id=dev, device_id_type=MESH)
+
+    for i in range(1, 4):
+        greet(at_z(lax.rem(z + i, 4)))
+        greet((s, lax.rem(t + i, 4)))
+    greet((z * 2 + y_far, t))
+    pl.semaphore_wait(barrier, 7)
+
+    def remote(src, dst, send, recv, dev):
+        return pltpu.make_async_remote_copy(
+            src_ref=src, dst_ref=dst, send_sem=send, recv_sem=recv,
+            device_id=dev, device_id_type=MESH)
+
+    def own_rows(block):
+        return pl.ds(pl.multiple_of(block * krows, 128), krows)
+
+    def pair_cols(p):
+        return pl.ds(pl.multiple_of(p * pair, 128), pair)
+
+    mine_rows = own_rows(zl * 2 + y)
+    near_rows = own_rows((1 - zl) * 2 + y)
+
+    def w_own(i):
+        return pltpu.make_async_copy(
+            weights[i].at[:, pair_cols(zl)], w_buf.at[i, mine_rows], w_local.at[i])
+
+    def w_over_z(i):
+        return remote(weights[i].at[:, pair_cols(1 - zl)], w_buf.at[i, mine_rows],
+                      w_send.at[0, i], w_recv.at[0, i], at_z(z_near))
+
+    def w_over_y(i):
+        return remote(weights[i].at[:, pair_cols(zl)], w_buf.at[i, mine_rows],
+                      w_send.at[1, i], w_recv.at[1, i], (z * 2 + y_far, t))
+
+    def w_relay(i):
+        return remote(w_buf.at[i, near_rows], w_buf.at[i, near_rows],
+                      w_send.at[2, i], w_recv.at[2, i], (z * 2 + y_far, t))
+
+    hold = 8
+
+    def slot(quarter, block):
+        return quarter * 4 + block
+
+    def x_swap():
+        there = jnp.where(1 - c == zh, slot(1 - x, z), hold)
+        return remote(act, x_buf.at[there], x_send.at[0], x_recv.at[there], (s, t_flip))
+
+    def x_here():
+        return jnp.where(hub, slot(x, z), hold)
+
+    def x_move(index, block, dev):
+        return remote(x_buf.at[block], x_buf.at[block], x_send.at[index], x_recv.at[block], dev)
+
+    def x_arrived(block):
+        remote(x_buf.at[block], x_buf.at[block], x_send.at[0], x_recv.at[block], (s, t)).wait_recv()
+
+    def x_cross():
+        dest = jnp.where(c == 0, 1, 2)
+        return remote(x_buf.at[hold], x_buf.at[slot(x, z)], x_send.at[1],
+                      x_recv.at[slot(x, z)], at_z(dest))
+
+    @pl.when(jnp.logical_not(straight))
+    def _():
+        x_swap().start()
+
+    @pl.when(straight)
+    def _():
+        pltpu.make_async_copy(act, x_buf.at[x_here()], local_sem).start()
+
+    for i in range(3):
+        w_own(i).start()
+    w_over_z(0).start()
+    w_over_y(0).start()
+
+    @pl.loop(0, 4)
+    def _(b):
+        rows = pl.ds(pl.multiple_of(b * tok, tok), tok)
+        half = HEAD // 2
+        lane = lax.broadcasted_iota(jnp.int32, (tok, 128), 1)
+        place = (b * 2 + y) * tok + lax.broadcasted_iota(jnp.int32, (tok, 128), 0)
+        exponent = lax.rem(lane, half).astype(jnp.float32) * (2.0 / HEAD)
+        angle = place.astype(jnp.float32) * jnp.exp(exponent * (-math.log(rope_base)))
+        cos_buf[rows, :] = jnp.cos(angle)
+        sine = jnp.sin(angle)
+        sin_buf[rows, :] = jnp.where(lax.rem(lane, HEAD) < half, -sine, sine)
+
+    @pl.when(straight)
+    def _():
+        pltpu.make_async_copy(act, x_buf.at[x_here()], local_sem).wait()
+
+    @pl.when(jnp.logical_not(straight))
+    def _():
+        x_arrived(x_here())
+
+    order = (z, z_near, jnp.where(inner, 3 - z, z_pair), jnp.where(inner, z_pair, 3 - z))
+    mine = jnp.where(hub, x, 1 - x)
+
+    @pl.when(hub)
+    def _():
+        x_move(1, slot(x, z), at_z(z_near)).start()
+
+    @pl.when(jnp.logical_not(hub))
+    def _():
+        x_cross().start()
+
+    w_over_z(1).start()
+    w_over_y(1).start()
+    w_over_z(0).wait_recv()
+    w_relay(0).start()
+    w_over_z(2).start()
+    w_over_y(2).start()
+
+    def c_copy(i, b):
+        return remote(c_buf.at[i, b], r_buf.at[i, b], c_send.at[i, b], c_recv.at[i, b], at_z(z_pair))
+
+    def part_sum(i, b):
+        total = jnp.dot(x_buf[b], w_buf[i, :feat, :], preferred_element_type=jnp.float32)
+        total = total + jnp.dot(x_buf[4 + b], w_buf[i, feat:, :], preferred_element_type=jnp.float32)
+        low = total[:, :width]
+        high = total[:, width:]
+        own_buf[i, b] = jnp.where(zh == 0, low, high)
+        give = jnp.where(zh == 0, high, low)
+        c_buf[i, b] = jnp.concatenate([give[:part], give[part:]], axis=1).astype(jnp.bfloat16)
+        c_copy(i, b).start()
+
+    def w_wait(i):
+        w_own(i).wait()
+        w_over_y(i).wait_recv()
+        w_relay(i).wait_recv()
+
+    for step in range(4):
+        b = order[step]
+
+        @pl.when(hub)
+        def _():
+            if step > 0:
+                x_arrived(slot(x, b))
+            x_move(2 + 2 * step, slot(x, b), (s, t_flip)).start()
+            x_move(3 + 2 * step, slot(x, b), (s, t_core)).start()
+            if step > 1:
+                @pl.when(inner)
+                def _():
+                    x_move(8 + step, slot(x, b), at_z(z_near)).start()
+
+        @pl.when(jnp.logical_not(hub))
+        def _():
+            x_arrived(slot(1 - x, b))
+            x_move(3 + 2 * step, slot(1 - x, b), (s, t_core)).start()
+
+        if step == 1:
+            w_over_z(1).wait_recv()
+            w_relay(1).start()
+        if step == 0:
+            w_wait(0)
+        x_arrived(slot(1 - mine, b))
+        part_sum(0, b)
+
+    w_wait(1)
+
+    @pl.loop(0, 4)
+    def _(i):
+        part_sum(1, lax.rem(zh * 2 + i, 4))
+
+    w_over_z(2).wait_recv()
+    w_relay(2).start()
+
+    most = SPAN * DILATIONS[-1]
+    kv_buf[0:most, :] = jnp.zeros((most, 2 * width), jnp.bfloat16)
+
+    def kv_rows(b, which):
+        return pl.ds(pl.multiple_of(most + (b * 2 + which) * tok, 128), tok)
+
+    def kv_copy(b):
+        rows = kv_rows(b, y)
+        return remote(kv_buf.at[rows], kv_buf.at[rows], kv_send.at[b], kv_recv.at[b],
+                      (z * 2 + y_far, t))
+
+    def kv_arrival(b):
+        rows = kv_rows(b, y_far)
+        return remote(kv_buf.at[rows], kv_buf.at[rows], kv_send.at[b], kv_recv.at[b],
+                      (z * 2 + y_far, t))
+
+    def whole_sum(i, b):
+        c_copy(i, b).wait_recv()
+        came = r_buf[i, b].astype(jnp.float32)
+        return own_buf[i, b] + jnp.concatenate([came[:, :width], came[:, width:]], axis=0)
+
+    def rotate(turn, b):
+        rows = pl.ds(pl.multiple_of(b * tok, tok), tok)
+        half = HEAD // 2
+        ahead = jnp.concatenate([turn[:, half:], turn[:, :half]], axis=1)
+        behind = jnp.concatenate([turn[:, -half:], turn[:, :-half]], axis=1)
+        lane = lax.broadcasted_iota(jnp.int32, turn.shape, 1)
+        other = jnp.where((lane & (HEAD - 1)) < half, ahead, behind)
+        cosine = jnp.concatenate([cos_buf[rows, :], cos_buf[rows, :HEAD]], axis=1)
+        sine = jnp.concatenate([sin_buf[rows, :], sin_buf[rows, :HEAD]], axis=1)
+        return (turn * cosine + other * sine).astype(jnp.bfloat16)
+
+    @pl.loop(0, 4)
+    def _(b):
+        rows = pl.ds(pl.multiple_of(b * tok, tok), tok)
+        q_buf[rows, :] = rotate(whole_sum(0, b), b)
+
+    w_wait(2)
+
+    @pl.loop(0, 4)
+    def _(b):
+        part_sum(2, b)
+
+    @pl.loop(0, 4)
+    def _(b):
+        kv_buf[kv_rows(b, y), :width] = rotate(whole_sum(1, b), b)
+
+    def gather_block(b):
+        kv_buf[kv_rows(b, y), width:] = whole_sum(2, b).astype(jnp.bfloat16)
+        kv_copy(b).start()
+
+    head = 2 * zl + zh
+
+    def m_copy(b):
+        return remote(o_buf.at[b], m_buf.at[head], m_send.at[b], m_recv.at[head], at_z(b))
+
+    def m_arrival(source):
+        return remote(m_buf.at[source], m_buf.at[source], m_send.at[source], m_recv.at[source], at_z(z))
+
+    def attend(b):
+        kv_arrival(b).wait_recv()
+        rows = pl.ds(pl.multiple_of(b * tok, tok), tok)
+        first = (b * 2 + y) * tok
+        mixed_list = []
+        total_list = []
+        for index, dilation in enumerate(DILATIONS):
+            reach = SPAN * dilation
+            keys = reach + tok
+            near = pl.ds(pl.multiple_of(most - reach + first, 128), keys)
+            q = q_buf[rows, index * HEAD:(index + 1) * HEAD]
+            k = kv_buf[near, index * HEAD:(index + 1) * HEAD]
+            v = kv_buf[near, width + index * HEAD:width + (index + 1) * HEAD]
+            scores = lax.dot_general(
+                q, k, (((1,), (1,)), ((), ())), preferred_element_type=jnp.float32
+            ) * HEAD ** (-0.5)
+            col = lax.broadcasted_iota(jnp.int32, (tok, keys), 1)
+            gap = reach + lax.broadcasted_iota(jnp.int32, (tok, keys), 0) - col
+            allowed = (gap >= 0) & (gap <= reach) & (col >= reach - first)
+            if dilation > 1:
+                allowed = allowed & ((gap & (dilation - 1)) == 0)
+            scores = jnp.where(allowed, scores, -jnp.inf)
+            row_max = jnp.max(scores, axis=1, keepdims=True)
+            expo = jnp.exp(scores - row_max)
+            denominator = jnp.sum(expo, axis=1, keepdims=True)
+            mixed = jnp.dot(expo.astype(jnp.bfloat16), v, preferred_element_type=jnp.float32)
+            mixed_list.append(mixed / denominator)
+            total_list.append(row_max + jnp.log(denominator))
+        peak = jnp.maximum(jnp.maximum(total_list[0], total_list[1]), total_list[2])
+        shifted = [jnp.exp(one - peak) for one in total_list]
+        whole = shifted[0] + shifted[1] + shifted[2]
+        merged = sum(a / whole * b_ for a, b_ in zip(shifted, mixed_list)).astype(jnp.bfloat16)
+
+        @pl.when(b != z)
+        def _():
+            o_buf[b] = merged
+            m_copy(b).start()
+
+        @pl.when(b == z)
+        def _():
+            m_buf[head] = merged
+
+    gather_block(0)
+
+    @pl.loop(1, 4)
+    def _(b):
+        gather_block(b)
+        attend(b - 1)
+
+    attend(3)
+
+    for i in range(1, 4):
+        source = lax.rem(z + i, 4)
+        m_arrival(2 * lax.rem(source, 2) + lax.div(source, 2)).wait_recv()
+    out[...] = jnp.concatenate(
+        [m_buf[h].astype(jnp.float32) for h in range(4)], axis=1).astype(jnp.bfloat16)
+
+    for i in range(1, 4):
+        m_copy(lax.rem(z + i, 4)).wait_send()
+
+    @pl.loop(0, 4)
+    def _(b):
+        kv_copy(b).wait_send()
+        for i in range(3):
+            c_copy(i, b).wait_send()
+
+    for i in range(3):
+        w_over_z(i).wait_send()
+        w_over_y(i).wait_send()
+        w_relay(i).wait_send()
+
+    @pl.when(jnp.logical_not(straight))
+    def _():
+        x_swap().wait_send()
+
+    @pl.when(jnp.logical_not(hub))
+    def _():
+        x_cross().wait_send()
+
+    @pl.when(hub)
+    def _():
+        x_move(1, slot(x, z), at_z(z_near)).wait_send()
+
+    for step in range(4):
+        b = order[step]
+
+        @pl.when(hub)
+        def _():
+            x_move(2 + 2 * step, slot(x, b), (s, t_flip)).wait_send()
+            x_move(3 + 2 * step, slot(x, b), (s, t_core)).wait_send()
+            if step > 1:
+                @pl.when(inner)
+                def _():
+                    x_move(8 + step, slot(x, b), at_z(z_near)).wait_send()
+
+        @pl.when(jnp.logical_not(hub))
+        def _():
+            x_move(3 + 2 * step, slot(1 - x, b), (s, t_core)).wait_send()
+
+
+def halves(activity, wq, wk, wv):
+    tok, feat = activity.shape
+    krows, col_width = wq.shape
+    width = col_width // 4
+    rows = 4 * tok
+    dma = pltpu.SemaphoreType.DMA
+    return pl.pallas_call(
+        halves_kernel,
+        out_shape=jax.ShapeDtypeStruct((tok, 4 * HEAD), jnp.bfloat16),
+        in_specs=[pl.BlockSpec(memory_space=pl.ANY)] * 4,
+        out_specs=pl.BlockSpec(memory_space=pltpu.VMEM),
+        scratch_shapes=[
+            pltpu.VMEM((9, tok, feat), jnp.bfloat16),
+            pltpu.VMEM((3, 4 * krows, 2 * width), jnp.bfloat16),
+            pltpu.VMEM((3, 4, tok, width), jnp.float32),
+            pltpu.VMEM((3, 4, tok // 2, 2 * width), jnp.bfloat16),
+            pltpu.VMEM((3, 4, tok // 2, 2 * width), jnp.bfloat16),
+            pltpu.VMEM((rows, width), jnp.bfloat16),
+            pltpu.VMEM((SPAN * DILATIONS[-1] + 2 * rows, 2 * width), jnp.bfloat16),
+            pltpu.VMEM((4, tok, HEAD), jnp.bfloat16),
+            pltpu.VMEM((4, tok, HEAD), jnp.bfloat16),
+            pltpu.VMEM((rows, 128), jnp.float32),
+            pltpu.VMEM((rows, 128), jnp.float32),
+            dma, dma((3,)), dma((12,)), dma((9,)), dma((3, 3)), dma((3, 3)),
+            dma((3, 4)), dma((3, 4)), dma((4,)), dma((4,)), dma((4,)), dma((4,)),
+        ],
+        compiler_params=pltpu.CompilerParams(
+            collective_id=2, has_side_effects=True, vmem_limit_bytes=58 * 2**20),
+        cost_estimate=pl.CostEstimate(
+            flops=2 * rows * feat * 3 * col_width, bytes_accessed=300 * 2**20, transcendentals=0),
+    )(activity, wq, wk, wv)
+
+
 def per_device(activity, query_weight, key_weight, value_weight, merge_weight):
     G = lax.axis_size("tp")
     R = lax.axis_size("sp") // G
     r = lax.axis_index("sp") % R
     tok = activity.shape[0]
     merge_full = lax.all_gather(merge_weight, "sp", axis=1, tiled=True)
+    if G == 4 and R == 2:
+        merged = halves(activity, query_weight, key_weight, value_weight)
+        return finish(merged, merge_full, 8)
     block_start = (jnp.arange(G, dtype=jnp.int32) * R + r) * tok
     pos = (block_start[:, None] + jnp.arange(tok, dtype=jnp.int32)[None, :]).reshape(G * tok)
     half = HEAD // 2

time: 225 us -> 185 us (0.82)
  Pallas kernels: 204 us -> 166 us
    pallas_call x1, Pallas kernels: 185 us -> 148 us  [halves(): pl.pallas_call(halves_kernel, out_shape=jax.ShapeDtypeStruct((tok, 4 * HE...]
  transfers between devices with their start and end apart: 1 -> 1, of which waited for: 0 -> 0; matrix products, arithmetic and copies ran while one was open for 1% -> 0% of each run, Pallas kernels for 82% -> 81%
where the time goes in v1:
time: 185 us; the launch traced here: 183 us
  Pallas kernels  166 us (90%)
  between operations  13.4 us (7%)
  local copies, waits for them, and re-layouts  3.28 us (2%)
    pallas_call x1, Pallas kernels, halves(): pl.pallas_call(halves_kernel, out_shape=jax.ShapeDtypeStruct((tok, 4 * HE...  148 us
    pallas_call x1, Pallas kernels, finish(): pl.pallas_call(finish_kernel, out_shape=jax.ShapeDtypeStruct((rows, weigh...  17.8 us
  transfers between devices with their start and end apart: 1, of which 0 were waited for; matrix products, arithmetic and copies ran while one was open for 0% of the time, Pallas kernels for 81%

profile of v1, /device:TPU:25, one launch (start us, length us, event | category | flops | bytes accessed | tf_op | source)
XLA Modules:
  0.0 183.1 jit_solution(2823579128984254878)
XLA Ops:
  6.5 0.0 all-gather.2.cloned.1.call-start
  6.5 0.7 all-gather.2.cloned.1.call-update
  7.3 147.9 %shard_map.55.merged = bf16[256,256]{1,0:T(8,128)(2,1)} custom-call(bf16[256,1024]{1,0:T(8,128)(2,1)} %act.1, bf16[512,768]{1,0:T(8,128)(2,1)} %wq.1, bf16[512,768]{1,0:T(8,128)(2,1)} %wk.1, bf16[512,768]{1,0:T(8,128)(2,1)} %wv.1), custom_call_target="tpu_custom_call" | custom-call | flops 4831838208 | bytes 314572800 | tf_op jit(solution)/shard_map/pallas_call | solution.py:778
  155.2 0.0 all-gather.2.cloned.1.call-done.weight
  155.2 0.0 copy-start
  155.2 1.6 copy-done
  156.8 0.0 copy-start.1
  156.8 0.9 copy-done.1
  157.7 17.8 %shard_map.56 = bf16[64,4096]{1,0:T(8,128)(2,1)S(1)} custom-call(bf16[256,256]{1,0:T(8,128)(2,1)S(1)} %copy-done.1, bf16[256,4096]{1,0:T(8,128)(2,1)S(1)} %copy-done), custom_call_target="tpu_custom_call" | custom-call | tf_op jit(solution)/shard_map/pallas_call | solution.py:393
  175.5 0.8 copy.7
Async XLA Ops:
  6.5 148.7 %all-gather.2.cloned.1.call-start = ((), (), s32[]{:S(2)}) async-start(), calls=%async_computation | async-start | bytes 2359296 | tf_op jit(solution)/shard_map/all_gather | solution.py:810
  155.2 1.6 copy-start
  156.8 0.9 copy-start.1
Sparse Core Ops, SparseCore 0:
  9.4 71.1 all-gather.1

commit v2 on v1

--- a/solution.py
+++ b/solution.py
@@ -409,10 +409,12 @@
 
 
 def halves_kernel(
-    act, wq, wk, wv, out,
+    act, wq, wk, wv, wm, out,
     x_buf, w_buf, own_buf, c_buf, r_buf, q_buf, kv_buf, o_buf, m_buf, cos_buf, sin_buf,
+    wm_buf, merged_buf, near_out, near_in, far_out, far_in, held,
     local_sem, w_local, x_send, x_recv, w_send, w_recv, c_send, c_recv,
-    kv_send, kv_recv, m_send, m_recv,
+    kv_send, kv_recv, m_send, m_recv, wm_local, wm_send, wm_recv,
+    near_send, near_recv, far_send, far_recv,
 ):
     s = lax.axis_index("sp")
     t = lax.axis_index("tp")
@@ -505,6 +507,21 @@
         return remote(x_buf.at[hold], x_buf.at[slot(x, z)], x_send.at[1],
                       x_recv.at[slot(x, z)], at_z(dest))
 
+    def wm_move(index, block, dev):
+        return remote(wm_buf.at[block], wm_buf.at[block], wm_send.at[index], wm_recv.at[block], dev)
+
+    def wm_first():
+        return remote(wm, wm_buf.at[s], wm_send.at[0], wm_recv.at[s], at_z(z_pair))
+
+    def wm_here():
+        return pltpu.make_async_copy(wm, wm_buf.at[s], wm_local)
+
+    y_dev = (z * 2 + y_far, t)
+    mate = z_pair * 2 + y
+    wm_pairs = (
+        (1, s, y_dev), (2, s, at_z(z_near)), (3, mate, y_dev), (4, mate, at_z(z_near)))
+    wm_last = ((5, z_near * 2 + y, y_dev), (6, z_pair * 2 + y_far, at_z(z_near)))
+
     @pl.when(jnp.logical_not(straight))
     def _():
         x_swap().start()
@@ -515,6 +532,8 @@
 
     for i in range(3):
         w_own(i).start()
+    wm_here().start()
+    wm_first().start()
     w_over_z(0).start()
     w_over_y(0).start()
 
@@ -541,20 +560,37 @@
     order = (z, z_near, jnp.where(inner, 3 - z, z_pair), jnp.where(inner, z_pair, 3 - z))
     mine = jnp.where(hub, x, 1 - x)
 
+    def x_hand_on(step):
+        block = slot(x, order[step])
+        x_move(2 + 2 * step, block, (s, t_flip)).start()
+        x_move(3 + 2 * step, block, (s, t_core)).start()
+        if step > 1:
+            @pl.when(inner)
+            def _():
+                x_move(8 + step, block, at_z(z_near)).start()
+
+    def hub_step(step):
+        x_arrived(slot(x, order[step]))
+        x_hand_on(step)
+
+    def spoke_step(step):
+        block = slot(1 - x, order[step])
+        x_arrived(block)
+        x_move(3 + 2 * step, block, (s, t_core)).start()
+
     @pl.when(hub)
     def _():
         x_move(1, slot(x, z), at_z(z_near)).start()
+        x_hand_on(0)
 
     @pl.when(jnp.logical_not(hub))
     def _():
         x_cross().start()
 
     w_over_z(1).start()
-    w_over_y(1).start()
     w_over_z(0).wait_recv()
     w_relay(0).start()
-    w_over_z(2).start()
-    w_over_y(2).start()
+    w_over_y(1).start()
 
     def c_copy(i, b):
         return remote(c_buf.at[i, b], r_buf.at[i, b], c_send.at[i, b], c_recv.at[i, b], at_z(z_pair))
@@ -574,41 +610,71 @@
         w_over_y(i).wait_recv()
         w_relay(i).wait_recv()
 
-    for step in range(4):
-        b = order[step]
-
-        @pl.when(hub)
-        def _():
-            if step > 0:
-                x_arrived(slot(x, b))
-            x_move(2 + 2 * step, slot(x, b), (s, t_flip)).start()
-            x_move(3 + 2 * step, slot(x, b), (s, t_core)).start()
-            if step > 1:
-                @pl.when(inner)
-                def _():
-                    x_move(8 + step, slot(x, b), at_z(z_near)).start()
-
-        @pl.when(jnp.logical_not(hub))
-        def _():
-            x_arrived(slot(1 - x, b))
-            x_move(3 + 2 * step, slot(1 - x, b), (s, t_core)).start()
-
-        if step == 1:
-            w_over_z(1).wait_recv()
-            w_relay(1).start()
-        if step == 0:
-            w_wait(0)
-        x_arrived(slot(1 - mine, b))
-        part_sum(0, b)
+    def other_arrived(step):
+        x_arrived(slot(1 - mine, order[step]))
+
+    spoke = jnp.logical_not(hub)
+    inner_hub = hub & inner
+    outer_hub = hub & jnp.logical_not(inner)
+
+    @pl.when(spoke)
+    def _():
+        spoke_step(0)
+
+    @pl.when(hub)
+    def _():
+        hub_step(1)
+
+    @pl.when(inner_hub)
+    def _():
+        hub_step(2)
+
+    w_wait(0)
+    other_arrived(0)
+    part_sum(0, order[0])
+
+    w_over_z(1).wait_recv()
+    w_relay(1).start()
+    w_over_y(2).start()
+
+    @pl.when(inner_hub)
+    def _():
+        hub_step(3)
+
+    w_over_z(2).start()
+
+    @pl.when(spoke)
+    def _():
+        spoke_step(1)
+
+    other_arrived(1)
+    part_sum(0, order[1])
+
+    @pl.when(spoke)
+    def _():
+        spoke_step(2)
+
+    @pl.when(outer_hub)
+    def _():
+        hub_step(2)
+        hub_step(3)
 
     w_wait(1)
-
-    @pl.loop(0, 4)
-    def _(i):
-        part_sum(1, lax.rem(zh * 2 + i, 4))
-
+    part_sum(1, order[0])
+    part_sum(1, order[1])
     w_over_z(2).wait_recv()
     w_relay(2).start()
+    other_arrived(2)
+    part_sum(0, order[2])
+    part_sum(1, order[2])
+
+    @pl.when(spoke)
+    def _():
+        spoke_step(3)
+
+    other_arrived(3)
+    part_sum(0, order[3])
+    part_sum(1, order[3])
 
     most = SPAN * DILATIONS[-1]
     kv_buf[0:most, :] = jnp.zeros((most, 2 * width), jnp.bfloat16)
@@ -648,6 +714,10 @@
         q_buf[rows, :] = rotate(whole_sum(0, b), b)
 
     w_wait(2)
+    wm_here().wait()
+    wm_move(0, mate, y_dev).wait_recv()
+    for index, block, dev in wm_pairs:
+        wm_move(index, block, dev).start()
 
     @pl.loop(0, 4)
     def _(b):
@@ -720,11 +790,72 @@
 
     attend(3)
 
+    def wm_came(block):
+        wm_move(0, block, y_dev).wait_recv()
+
+    wm_came(z_near * 2 + y)
+    wm_came(z_pair * 2 + y_far)
+    for index, block, dev in wm_last:
+        wm_move(index, block, dev).start()
+
     for i in range(1, 4):
         source = lax.rem(z + i, 4)
         m_arrival(2 * lax.rem(source, 2) + lax.div(source, 2)).wait_recv()
-    out[...] = jnp.concatenate(
+    merged_buf[...] = jnp.concatenate(
         [m_buf[h].astype(jnp.float32) for h in range(4)], axis=1).astype(jnp.bfloat16)
+
+    far = lax.rem(t + 2, 4)
+    across = 3 - t
+    piece = out.shape[0]
+    cols = wm.shape[1]
+
+    def near_copy(n):
+        return remote(near_out.at[n], near_in.at[n], near_send.at[n], near_recv.at[n], (s, t_core))
+
+    def far_copy(n):
+        return remote(far_out.at[n], far_in.at[n], far_send.at[n], far_recv.at[n], (s, far))
+
+    chunks = (s, mate, z * 2 + y_far, z_near * 2 + y, z_pair * 2 + y_far,
+              lax.rem(z_near + 2, 4) * 2 + y,
+              z_near * 2 + y_far, lax.rem(z_near + 2, 4) * 2 + y_far)
+
+    def product(n):
+        def rows_of(owner):
+            picked = merged_buf[pl.ds(pl.multiple_of(owner * piece, piece), piece), :]
+            return jnp.dot(picked, wm_buf[chunks[n]], preferred_element_type=jnp.float32)
+        near_out[n, 0] = rows_of(across).astype(jnp.bfloat16)
+        near_out[n, 1] = rows_of(t_core).astype(jnp.bfloat16)
+        near_copy(n).start()
+        held[n, 0] = rows_of(far)
+        held[n, 1] = rows_of(t)
+
+    def pass_on(n):
+        near_copy(n).wait_recv()
+        far_out[n] = (held[n, 0] + near_in[n, 0].astype(jnp.float32)).astype(jnp.bfloat16)
+        far_copy(n).start()
+        held[n, 1] = held[n, 1] + near_in[n, 1].astype(jnp.float32)
+
+    for n in range(8):
+        if n == 2:
+            wm_came(chunks[2])
+        if n > 4:
+            wm_came(chunks[n])
+        product(n)
+        if n > 0:
+            pass_on(n - 1)
+    pass_on(7)
+
+    for n in range(8):
+        far_copy(n).wait_recv()
+        at = pl.ds(pl.multiple_of(chunks[n] * cols, 128), cols)
+        out[:, at] = (held[n, 1] + far_in[n].astype(jnp.float32)).astype(jnp.bfloat16)
+
+    for n in range(8):
+        near_copy(n).wait_send()
+        far_copy(n).wait_send()
+    wm_first().wait_send()
+    for index, block, dev in wm_pairs + wm_last:
+        wm_move(index, block, dev).wait_send()
 
     for i in range(1, 4):
         m_copy(lax.rem(z + i, 4)).wait_send()
@@ -769,16 +900,18 @@
             x_move(3 + 2 * step, slot(1 - x, b), (s, t_core)).wait_send()
 
 
-def halves(activity, wq, wk, wv):
+def halves(activity, wq, wk, wv, wm):
     tok, feat = activity.shape
     krows, col_width = wq.shape
     width = col_width // 4
     rows = 4 * tok
+    piece = tok // 4
+    cols = wm.shape[1]
     dma = pltpu.SemaphoreType.DMA
     return pl.pallas_call(
         halves_kernel,
-        out_shape=jax.ShapeDtypeStruct((tok, 4 * HEAD), jnp.bfloat16),
-        in_specs=[pl.BlockSpec(memory_space=pl.ANY)] * 4,
+        out_shape=jax.ShapeDtypeStruct((piece, 8 * cols), jnp.bfloat16),
+        in_specs=[pl.BlockSpec(memory_space=pl.ANY)] * 5,
         out_specs=pl.BlockSpec(memory_space=pltpu.VMEM),
         scratch_shapes=[
             pltpu.VMEM((9, tok, feat), jnp.bfloat16),
@@ -792,14 +925,22 @@
             pltpu.VMEM((4, tok, HEAD), jnp.bfloat16),
             pltpu.VMEM((rows, 128), jnp.float32),
             pltpu.VMEM((rows, 128), jnp.float32),
+            pltpu.VMEM((8, tok, cols), jnp.bfloat16),
+            pltpu.VMEM((tok, 4 * HEAD), jnp.bfloat16),
+            pltpu.VMEM((8, 2, piece, cols), jnp.bfloat16),
+            pltpu.VMEM((8, 2, piece, cols), jnp.bfloat16),
+            pltpu.VMEM((8, piece, cols), jnp.bfloat16),
+            pltpu.VMEM((8, piece, cols), jnp.bfloat16),
+            pltpu.VMEM((8, 2, piece, cols), jnp.float32),
             dma, dma((3,)), dma((12,)), dma((9,)), dma((3, 3)), dma((3, 3)),
             dma((3, 4)), dma((3, 4)), dma((4,)), dma((4,)), dma((4,)), dma((4,)),
+            dma, dma((7,)), dma((8,)), dma((8,)), dma((8,)), dma((8,)), dma((8,)),
         ],
         compiler_params=pltpu.CompilerParams(
             collective_id=2, has_side_effects=True, vmem_limit_bytes=58 * 2**20),
         cost_estimate=pl.CostEstimate(
             flops=2 * rows * feat * 3 * col_width, bytes_accessed=300 * 2**20, transcendentals=0),
-    )(activity, wq, wk, wv)
+    )(activity, wq, wk, wv, wm)
 
 
 def per_device(activity, query_weight, key_weight, value_weight, merge_weight):
@@ -807,10 +948,9 @@
     R = lax.axis_size("sp") // G
     r = lax.axis_index("sp") % R
     tok = activity.shape[0]
+    if G == 4 and R == 2:
+        return halves(activity, query_weight, key_weight, value_weight, merge_weight)
     merge_full = lax.all_gather(merge_weight, "sp", axis=1, tiled=True)
-    if G == 4 and R == 2:
-        merged = halves(activity, query_weight, key_weight, value_weight)
-        return finish(merged, merge_full, 8)
     block_start = (jnp.arange(G, dtype=jnp.int32) * R + r) * tok
     pos = (block_start[:, None] + jnp.arange(tok, dtype=jnp.int32)[None, :]).reshape(G * tok)
     half = HEAD // 2

time: 185 us -> 134 us (0.72); the launches traced: 183 us -> 134 us
  Pallas kernels: 166 us -> 132 us
  between operations: 13.4 us -> 0.01 us
    pallas_call x2 -> x1, Pallas kernels: 166 us -> 132 us  [halves(): pl.pallas_call(halves_kernel, out_shape=jax.ShapeDtypeStruct((piece, 8 *...]
  transfers between devices with their start and end apart: 1 -> 0, of which waited for: 0 -> 0; matrix products, arithmetic and copies ran while one was open for 0% -> 0% of each run, Pallas kernels for 81% -> 0%
where the time goes in v2:
time: 134 us
  Pallas kernels  132 us (99%)
  local copies, waits for them, and re-layouts  1.87 us (1%)
    pallas_call x1, Pallas kernels, halves(): pl.pallas_call(halves_kernel, out_shape=jax.ShapeDtypeStruct((piece, 8 *...  132 us

profile of v2, /device:TPU:25, one launch (start us, length us, event | category | flops | bytes accessed | tf_op | source)
XLA Modules:
  0.0 134.2 jit_solution(13163720258732650445)
XLA Ops:
  0.0 132.3 %shard_map.55 = bf16[64,4096]{1,0:T(8,128)(2,1)} custom-call(bf16[256,1024]{1,0:T(8,128)(2,1)} %act.1, bf16[512,768]{1,0:T(8,128)(2,1)} %wq.1, bf16[512,768]{1,0:T(8,128)(2,1)} %wk.1, bf16[512,768]{1,0:T(8,128)(2,1)} %wv.1, bf16[256,512]{1,0:T(8,128)(2,1)} %wm.1), custom_call_target="tpu_custom_call" | custom-call | flops 4831838208 | bytes 314572800 | tf_op jit(solution)/shard_map/pallas_call | solution.py:911
  132.3 1.9 %copy.7 = bf16[64,4096]{1,0:T(8,128)(2,1)} copy(bf16[64,4096]{1,0:T(8,128)(2,1)} %shard_map.55) | data formatting | bytes 1048576

commit v3 on v1

--- a/solution.py
+++ b/solution.py
@@ -409,10 +409,13 @@
 
 
 def halves_kernel(
-    act, wq, wk, wv, out,
-    x_buf, w_buf, own_buf, c_buf, r_buf, q_buf, kv_buf, o_buf, m_buf, cos_buf, sin_buf,
+    act, wq, wk, wv, wm, out,
+    x_buf, w_buf, own_buf, c_buf, r_buf, q_buf, kv_buf, ky_out, ky_in, o_buf, m_buf,
+    cos_buf, sin_buf, wm_buf, merged_buf, near_out, near_in, far_out, far_in, held,
+    done_out,
     local_sem, w_local, x_send, x_recv, w_send, w_recv, c_send, c_recv,
-    kv_send, kv_recv, m_send, m_recv,
+    ky_send, ky_recv, m_send, m_recv, wm_local, wm_send, wm_recv,
+    near_send, near_recv, far_send, far_recv, done_send, done_recv,
 ):
     s = lax.axis_index("sp")
     t = lax.axis_index("tp")
@@ -422,21 +425,24 @@
     c = lax.rem(t, 2)
     zh = lax.div(z, 2)
     zl = lax.rem(z, 2)
-    G = 4
     tok, feat = act.shape
     krows = wq.shape[0]
     pair = wq.shape[1] // 2
     width = pair // 2
     part = tok // 2
-    weights = (wq, wk, wv)
+    weights = (wk, wq, wv)
     z_near = z + 1 - 2 * zl
     z_pair = lax.rem(z + 2, 4)
     y_far = 1 - y
+    y_dev = (z * 2 + y_far, t)
     t_flip = 3 - t
     t_core = t + 1 - 2 * c
     hub = c == zh
+    spoke = jnp.logical_not(hub)
     inner = zl != zh
+    outer = jnp.logical_not(inner)
     straight = c == x
+    bent = jnp.logical_not(straight)
 
     def at_z(other):
         return (other * 2 + y, t)
@@ -449,8 +455,13 @@
     for i in range(1, 4):
         greet(at_z(lax.rem(z + i, 4)))
         greet((s, lax.rem(t + i, 4)))
-    greet((z * 2 + y_far, t))
-    pl.semaphore_wait(barrier, 7)
+    greet(y_dev)
+    cross_z = jnp.where(c == 0, 1, 2)
+    cross_dev = (cross_z * 2 + y, t_core)
+
+    for i in range(1, 4):
+        greet((lax.rem(z + i, 4) * 2 + y, t_core))
+    pl.semaphore_wait(barrier, 10)
 
     def remote(src, dst, send, recv, dev):
         return pltpu.make_async_remote_copy(
@@ -476,201 +487,323 @@
 
     def w_over_y(i):
         return remote(weights[i].at[:, pair_cols(zl)], w_buf.at[i, mine_rows],
-                      w_send.at[1, i], w_recv.at[1, i], (z * 2 + y_far, t))
+                      w_send.at[1, i], w_recv.at[1, i], y_dev)
 
     def w_relay(i):
         return remote(w_buf.at[i, near_rows], w_buf.at[i, near_rows],
-                      w_send.at[2, i], w_recv.at[2, i], (z * 2 + y_far, t))
-
-    hold = 8
-
-    def slot(quarter, block):
-        return quarter * 4 + block
-
-    def x_swap():
-        there = jnp.where(1 - c == zh, slot(1 - x, z), hold)
-        return remote(act, x_buf.at[there], x_send.at[0], x_recv.at[there], (s, t_flip))
-
-    def x_here():
-        return jnp.where(hub, slot(x, z), hold)
-
-    def x_move(index, block, dev):
-        return remote(x_buf.at[block], x_buf.at[block], x_send.at[index], x_recv.at[block], dev)
-
-    def x_arrived(block):
-        remote(x_buf.at[block], x_buf.at[block], x_send.at[0], x_recv.at[block], (s, t)).wait_recv()
-
-    def x_cross():
-        dest = jnp.where(c == 0, 1, 2)
-        return remote(x_buf.at[hold], x_buf.at[slot(x, z)], x_send.at[1],
-                      x_recv.at[slot(x, z)], at_z(dest))
-
-    @pl.when(jnp.logical_not(straight))
-    def _():
-        x_swap().start()
-
-    @pl.when(straight)
-    def _():
-        pltpu.make_async_copy(act, x_buf.at[x_here()], local_sem).start()
-
-    for i in range(3):
-        w_own(i).start()
-    w_over_z(0).start()
-    w_over_y(0).start()
-
-    @pl.loop(0, 4)
-    def _(b):
-        rows = pl.ds(pl.multiple_of(b * tok, tok), tok)
-        half = HEAD // 2
-        lane = lax.broadcasted_iota(jnp.int32, (tok, 128), 1)
-        place = (b * 2 + y) * tok + lax.broadcasted_iota(jnp.int32, (tok, 128), 0)
-        exponent = lax.rem(lane, half).astype(jnp.float32) * (2.0 / HEAD)
-        angle = place.astype(jnp.float32) * jnp.exp(exponent * (-math.log(rope_base)))
-        cos_buf[rows, :] = jnp.cos(angle)
-        sine = jnp.sin(angle)
-        sin_buf[rows, :] = jnp.where(lax.rem(lane, HEAD) < half, -sine, sine)
-
-    @pl.when(straight)
-    def _():
-        pltpu.make_async_copy(act, x_buf.at[x_here()], local_sem).wait()
-
-    @pl.when(jnp.logical_not(straight))
-    def _():
-        x_arrived(x_here())
-
-    order = (z, z_near, jnp.where(inner, 3 - z, z_pair), jnp.where(inner, z_pair, 3 - z))
-    mine = jnp.where(hub, x, 1 - x)
-
-    @pl.when(hub)
-    def _():
-        x_move(1, slot(x, z), at_z(z_near)).start()
-
-    @pl.when(jnp.logical_not(hub))
-    def _():
-        x_cross().start()
-
-    w_over_z(1).start()
-    w_over_y(1).start()
-    w_over_z(0).wait_recv()
-    w_relay(0).start()
-    w_over_z(2).start()
-    w_over_y(2).start()
-
-    def c_copy(i, b):
-        return remote(c_buf.at[i, b], r_buf.at[i, b], c_send.at[i, b], c_recv.at[i, b], at_z(z_pair))
-
-    def part_sum(i, b):
-        total = jnp.dot(x_buf[b], w_buf[i, :feat, :], preferred_element_type=jnp.float32)
-        total = total + jnp.dot(x_buf[4 + b], w_buf[i, feat:, :], preferred_element_type=jnp.float32)
-        low = total[:, :width]
-        high = total[:, width:]
-        own_buf[i, b] = jnp.where(zh == 0, low, high)
-        give = jnp.where(zh == 0, high, low)
-        c_buf[i, b] = jnp.concatenate([give[:part], give[part:]], axis=1).astype(jnp.bfloat16)
-        c_copy(i, b).start()
+                      w_send.at[2, i], w_recv.at[2, i], y_dev)
 
     def w_wait(i):
         w_own(i).wait()
         w_over_y(i).wait_recv()
         w_relay(i).wait_recv()
 
-    for step in range(4):
-        b = order[step]
-
+    wm_slot = zl * 2 + y
+    wm_near_slot = (1 - zl) * 2 + y
+
+    def wm_here():
+        return pltpu.make_async_copy(wm, wm_buf.at[wm_slot], wm_local)
+
+    def wm_over_z():
+        return remote(wm, wm_buf.at[wm_slot], wm_send.at[0], wm_recv.at[wm_slot], at_z(z_near))
+
+    def wm_over_y():
+        return remote(wm, wm_buf.at[wm_slot], wm_send.at[1], wm_recv.at[wm_slot], y_dev)
+
+    def wm_relay():
+        return remote(wm_buf.at[wm_near_slot], wm_buf.at[wm_near_slot],
+                      wm_send.at[2], wm_recv.at[wm_near_slot], y_dev)
+
+    def wm_came(block):
+        remote(wm_buf.at[block], wm_buf.at[block], wm_send.at[0], wm_recv.at[block], y_dev).wait_recv()
+
+    hold = 8
+    order = (z, z_near, jnp.where(inner, 3 - z, z_pair), jnp.where(inner, z_pair, 3 - z))
+
+    def slot(quarter, block):
+        return quarter * 4 + block
+
+    def x_swap():
+        there = jnp.where(1 - c == zh, slot(1 - x, z), hold)
+        return remote(act, x_buf.at[there], x_send.at[0], x_recv.at[there], (s, t_flip))
+
+    def x_here():
+        return jnp.where(hub, slot(x, z), hold)
+
+    def x_local():
+        return pltpu.make_async_copy(act, x_buf.at[x_here()], local_sem)
+
+    def x_move(index, block, dev):
+        return remote(x_buf.at[block], x_buf.at[block], x_send.at[index], x_recv.at[block], dev)
+
+    def x_arrived(block):
+        remote(x_buf.at[block], x_buf.at[block], x_send.at[0], x_recv.at[block], (s, t)).wait_recv()
+
+    def x_near():
+        return x_move(1, slot(x, z), at_z(z_near))
+
+    def x_cross():
+        return remote(x_buf.at[hold], x_buf.at[slot(x, z)], x_send.at[1],
+                      x_recv.at[slot(x, z)], cross_dev)
+
+    def x_sideways(step):
+        return x_move(2 + 2 * step, slot(x, order[step]), (s, t_flip))
+
+    def x_inside(step):
+        return x_move(3 + 2 * step, slot(x, order[step]), (s, t_core))
+
+    def x_back(step):
+        return x_move(3 + 2 * step, slot(1 - x, order[step]), (s, t_core))
+
+    def x_outward(step):
+        return x_move(8 + step, slot(x, order[step]), at_z(z_near))
+
+    def lead(step):
+        if step > 0:
+            x_arrived(slot(x, order[step]))
+        if step > 1:
+            @pl.when(inner)
+            def _():
+                x_outward(step).start()
+        x_sideways(step).start()
+        x_inside(step).start()
+
+    def follow(step):
+        x_arrived(slot(1 - x, order[step]))
+        x_back(step).start()
+
+    def other_arrived(step):
+        leads = hub if step < 2 else spoke
+        x_arrived(slot(jnp.where(leads, 1 - x, x), order[step]))
+
+    def packed(rows):
+        return jnp.concatenate([rows[:part], rows[part:]], axis=1)
+
+    def c_copy(i, b):
+        return remote(c_buf.at[i, b], r_buf.at[i, b], c_send.at[i, b], c_recv.at[i, b], at_z(z_pair))
+
+    def part_sum(i, b, held_back):
+        total = jnp.dot(x_buf[b], w_buf[i, :feat, :], preferred_element_type=jnp.float32)
+        total = total + jnp.dot(x_buf[4 + b], w_buf[i, feat:, :], preferred_element_type=jnp.float32)
+        low = packed(total[:, :width])
+        high = packed(total[:, width:])
+        own_buf[i, b] = jnp.where(zh == 0, low, high)
+        c_buf[i, b] = jnp.where(zh == 0, high, low).astype(jnp.bfloat16)
+        if not held_back:
+            c_copy(i, b).start()
+        else:
+            @pl.when(outer)
+            def _():
+                c_copy(i, b).start()
+
+    w_over_z(0).start()
+    w_over_y(0).start()
+
+    @pl.when(bent)
+    def _():
+        x_swap().start()
+
+    @pl.when(straight)
+    def _():
+        x_local().start()
+
+    for i in range(3):
+        w_own(i).start()
+    wm_here().start()
+
+    def x_first():
         @pl.when(hub)
         def _():
-            if step > 0:
-                x_arrived(slot(x, b))
-            x_move(2 + 2 * step, slot(x, b), (s, t_flip)).start()
-            x_move(3 + 2 * step, slot(x, b), (s, t_core)).start()
-            if step > 1:
-                @pl.when(inner)
-                def _():
-                    x_move(8 + step, slot(x, b), at_z(z_near)).start()
-
-        @pl.when(jnp.logical_not(hub))
+            x_near().start()
+            lead(0)
+            w_over_z(1).start()
+            w_over_z(2).start()
+
+        @pl.when(spoke)
         def _():
-            x_arrived(slot(1 - x, b))
-            x_move(3 + 2 * step, slot(1 - x, b), (s, t_core)).start()
-
-        if step == 1:
-            w_over_z(1).wait_recv()
-            w_relay(1).start()
-        if step == 0:
-            w_wait(0)
-        x_arrived(slot(1 - mine, b))
-        part_sum(0, b)
+            x_cross().start()
+            w_over_z(1).start()
+
+    @pl.when(straight)
+    def _():
+        x_local().wait()
+        x_first()
+
+    @pl.loop(0, 4)
+    def _(b):
+        half = HEAD // 2
+        shape = (part, pair)
+        lane = lax.broadcasted_iota(jnp.int32, shape, 1)
+        place = (b * 2 + y) * tok + lax.broadcasted_iota(jnp.int32, shape, 0)
+        place = place + jnp.where(lane < width, 0, part)
+        exponent = (lane & (half - 1)).astype(jnp.float32) * (2.0 / HEAD)
+        angle = place.astype(jnp.float32) * jnp.exp(exponent * (-math.log(rope_base)))
+        cos_buf[b] = jnp.cos(angle)
+        sine = jnp.sin(angle)
+        sin_buf[b] = jnp.where((lane & (HEAD - 1)) < half, -sine, sine)
+
+    @pl.when(bent)
+    def _():
+        x_arrived(x_here())
+        x_first()
+
+    w_over_z(0).wait_recv()
+    w_relay(0).start()
+    w_over_y(1).start()
+
+    @pl.when(spoke)
+    def _():
+        follow(0)
+
+        @pl.when(inner)
+        def _():
+            lead(2)
+
+    @pl.when(hub)
+    def _():
+        lead(1)
+
+    w_wait(0)
+    other_arrived(0)
+    part_sum(0, order[0], False)
+
+    w_over_z(1).wait_recv()
+    w_relay(1).start()
+    w_over_y(2).start()
+
+    @pl.when(spoke)
+    def _():
+        @pl.when(inner)
+        def _():
+            lead(3)
+
+        w_over_z(2).start()
+        follow(1)
+
+    @pl.when(hub & inner)
+    def _():
+        follow(2)
+
+    other_arrived(1)
+    part_sum(0, order[1], False)
+
+    @pl.when(spoke & outer)
+    def _():
+        lead(2)
+
+    @pl.when(hub & inner)
+    def _():
+        follow(3)
 
     w_wait(1)
-
-    @pl.loop(0, 4)
-    def _(i):
-        part_sum(1, lax.rem(zh * 2 + i, 4))
+    part_sum(1, order[0], True)
+    part_sum(1, order[1], True)
+
+    @pl.when(spoke & outer)
+    def _():
+        lead(3)
+
+    @pl.when(hub & outer)
+    def _():
+        follow(2)
 
     w_over_z(2).wait_recv()
     w_relay(2).start()
+    other_arrived(2)
+    part_sum(0, order[2], True)
+    part_sum(1, order[2], True)
+
+    @pl.when(hub & outer)
+    def _():
+        follow(3)
+
+    other_arrived(3)
+    part_sum(0, order[3], True)
+    part_sum(1, order[3], True)
+
+    w_over_z(2).wait_send()
+    wm_over_z().start()
+    wm_over_y().start()
+
+    @pl.when(inner)
+    def _():
+        for i in range(2):
+            for step in range(4):
+                if i == 1 or step > 1:
+                    c_copy(i, order[step]).start()
 
     most = SPAN * DILATIONS[-1]
     kv_buf[0:most, :] = jnp.zeros((most, 2 * width), jnp.bfloat16)
 
+    w_wait(2)
+
+    @pl.loop(0, 4)
+    def _(b):
+        part_sum(2, b, False)
+
     def kv_rows(b, which):
         return pl.ds(pl.multiple_of(most + (b * 2 + which) * tok, 128), tok)
 
-    def kv_copy(b):
-        rows = kv_rows(b, y)
-        return remote(kv_buf.at[rows], kv_buf.at[rows], kv_send.at[b], kv_recv.at[b],
-                      (z * 2 + y_far, t))
-
-    def kv_arrival(b):
-        rows = kv_rows(b, y_far)
-        return remote(kv_buf.at[rows], kv_buf.at[rows], kv_send.at[b], kv_recv.at[b],
-                      (z * 2 + y_far, t))
+    def ky_copy(i, b):
+        return remote(ky_out.at[i, b], ky_in.at[i, b], ky_send.at[i, b], ky_recv.at[i, b], y_dev)
 
     def whole_sum(i, b):
         c_copy(i, b).wait_recv()
-        came = r_buf[i, b].astype(jnp.float32)
-        return own_buf[i, b] + jnp.concatenate([came[:, :width], came[:, width:]], axis=0)
+        return own_buf[i, b] + r_buf[i, b].astype(jnp.float32)
+
+    def unpacked(both):
+        return jnp.concatenate([both[:, :width], both[:, width:]], axis=0)
 
     def rotate(turn, b):
-        rows = pl.ds(pl.multiple_of(b * tok, tok), tok)
         half = HEAD // 2
         ahead = jnp.concatenate([turn[:, half:], turn[:, :half]], axis=1)
         behind = jnp.concatenate([turn[:, -half:], turn[:, :-half]], axis=1)
         lane = lax.broadcasted_iota(jnp.int32, turn.shape, 1)
         other = jnp.where((lane & (HEAD - 1)) < half, ahead, behind)
-        cosine = jnp.concatenate([cos_buf[rows, :], cos_buf[rows, :HEAD]], axis=1)
-        sine = jnp.concatenate([sin_buf[rows, :], sin_buf[rows, :HEAD]], axis=1)
-        return (turn * cosine + other * sine).astype(jnp.bfloat16)
-
-    @pl.loop(0, 4)
-    def _(b):
+        return (turn * cos_buf[b] + other * sin_buf[b]).astype(jnp.bfloat16)
+
+    theirs = (z_pair, lax.rem(z_near + 2, 4), jnp.where(outer, 3 - z_pair, z), jnp.where(outer, z, 3 - z_pair))
+
+    for step in range(4):
+        b = theirs[step]
+        turned = rotate(whole_sum(0, b), b)
+        ky_out[0, b] = turned
+        ky_copy(0, b).start()
+        kv_buf[kv_rows(b, y), :width] = unpacked(turned)
+
+    wm_came(wm_near_slot)
+    wm_relay().start()
+
+    for step in range(4):
+        b = theirs[step]
         rows = pl.ds(pl.multiple_of(b * tok, tok), tok)
-        q_buf[rows, :] = rotate(whole_sum(0, b), b)
-
-    w_wait(2)
-
-    @pl.loop(0, 4)
-    def _(b):
-        part_sum(2, b)
-
-    @pl.loop(0, 4)
-    def _(b):
-        kv_buf[kv_rows(b, y), :width] = rotate(whole_sum(1, b), b)
-
-    def gather_block(b):
-        kv_buf[kv_rows(b, y), width:] = whole_sum(2, b).astype(jnp.bfloat16)
-        kv_copy(b).start()
+        q_buf[rows, :] = unpacked(rotate(whole_sum(1, b), b))
+
+    def gather_values(b):
+        value = whole_sum(2, b).astype(jnp.bfloat16)
+        ky_out[1, b] = value
+        ky_copy(1, b).start()
+        kv_buf[kv_rows(b, y), width:] = unpacked(value)
+
+    def values_arrived(b):
+        ky_copy(0, b).wait_recv()
+        kv_buf[kv_rows(b, y_far), :width] = unpacked(ky_in[0, b])
+        ky_copy(1, b).wait_recv()
+        kv_buf[kv_rows(b, y_far), width:] = unpacked(ky_in[1, b])
 
     head = 2 * zl + zh
 
-    def m_copy(b):
-        return remote(o_buf.at[b], m_buf.at[head], m_send.at[b], m_recv.at[head], at_z(b))
-
-    def m_arrival(source):
-        return remote(m_buf.at[source], m_buf.at[source], m_send.at[source], m_recv.at[source], at_z(z))
+    def m_copy(b, there):
+        where = lax.rem(b + 2 * there, 4)
+        return remote(o_buf.at[b], m_buf.at[there, head], m_send.at[there, b],
+                      m_recv.at[there, head], at_z(where))
+
+    def m_arrival(there, source):
+        return remote(m_buf.at[there, source], m_buf.at[there, source], m_send.at[there, source],
+                      m_recv.at[there, source], at_z(z))
 
     def attend(b):
-        kv_arrival(b).wait_recv()
+        values_arrived(b)
         rows = pl.ds(pl.multiple_of(b * tok, tok), tok)
         first = (b * 2 + y) * tok
         mixed_list = []
@@ -701,105 +834,217 @@
         shifted = [jnp.exp(one - peak) for one in total_list]
         whole = shifted[0] + shifted[1] + shifted[2]
         merged = sum(a / whole * b_ for a, b_ in zip(shifted, mixed_list)).astype(jnp.bfloat16)
-
-        @pl.when(b != z)
-        def _():
-            o_buf[b] = merged
-            m_copy(b).start()
-
-        @pl.when(b == z)
-        def _():
-            m_buf[head] = merged
-
-    gather_block(0)
-
-    @pl.loop(1, 4)
+        o_buf[b] = merged
+        for there in range(2):
+            mine = lax.rem(b + 2 * there, 4) == z
+
+            @pl.when(jnp.logical_not(mine))
+            def _():
+                m_copy(b, there).start()
+
+            @pl.when(mine)
+            def _():
+                m_buf[there, head] = merged
+
+    gather_values(0)
+
+    gather_values(1)
+
+    @pl.loop(2, 4)
     def _(b):
-        gather_block(b)
-        attend(b - 1)
-
+        gather_values(b)
+        attend(b - 2)
+
+    wm_here().wait()
+
+    far = lax.rem(t + 2, 4)
+    across = 3 - t
+    piece = out.shape[0]
+    cols = wm.shape[1]
+
+    def near_copy(n):
+        return remote(near_out.at[n], near_in.at[n], near_send.at[n], near_recv.at[n], (s, t_core))
+
+    def far_copy(n):
+        return remote(far_out.at[n], far_in.at[n], far_send.at[n], far_recv.at[n], (s, far))
+
+    blocks = (wm_slot, wm_near_slot, zl * 2 + y_far, (1 - zl) * 2 + y_far)
+
+    def goes_over(n):
+        return zh == 1 - n // 4
+
+    def product(n):
+        there = zh if n < 4 else 1 - zh
+        block = blocks[n % 4]
+
+        def rows_of(owner):
+            picked = merged_buf[there, pl.ds(pl.multiple_of(owner * piece, piece), piece), :]
+            return jnp.dot(picked, wm_buf[block], preferred_element_type=jnp.float32)
+        near_out[n, 0] = rows_of(across).astype(jnp.bfloat16)
+        near_out[n, 1] = rows_of(t_core).astype(jnp.bfloat16)
+        near_copy(n).start()
+        held[n, 0] = rows_of(far)
+        held[n, 1] = rows_of(t)
+
+    def pass_on(n):
+        near_copy(n).wait_recv()
+        far_out[n] = (held[n, 0] + near_in[n, 0].astype(jnp.float32)).astype(jnp.bfloat16)
+        far_copy(n).start()
+        held[n, 1] = held[n, 1] + near_in[n, 1].astype(jnp.float32)
+
+    def total_of(n):
+        far_copy(n).wait_recv()
+        return (held[n, 1] + far_in[n].astype(jnp.float32)).astype(jnp.bfloat16)
+
+    def block_at(half, n):
+        return pl.ds(pl.multiple_of((half * 4 + blocks[n]) * cols, 128), cols)
+
+    def done_copy(n):
+        return remote(done_out.at[n], out.at[:, block_at(zh, n)], done_send.at[n],
+                      done_recv.at[n], at_z(z_pair))
+
+    def collect(group):
+        there = zh if group == 0 else 1 - zh
+        for i in range(1, 4):
+            source = lax.rem(z + i, 4)
+            m_arrival(there, 2 * lax.rem(source, 2) + lax.div(source, 2)).wait_recv()
+        merged_buf[there] = jnp.concatenate(
+            [m_buf[there, h].astype(jnp.float32) for h in range(4)], axis=1).astype(jnp.bfloat16)
+
+    def project_out(group):
+        collect(group)
+        for n in range(4 * group, 4 * group + 4):
+            if n == 2:
+                wm_came(blocks[2])
+            if n == 3:
+                wm_came(blocks[3])
+            product(n)
+            if n > 4 * group:
+                pass_on(n - 1)
+        pass_on(4 * group + 3)
+
+    def settle(group):
+        for n in range(4):
+            total = total_of(4 * group + n)
+
+            @pl.when(goes_over(4 * group))
+            def _():
+                done_out[n] = total
+                done_copy(n).start()
+
+            @pl.when(jnp.logical_not(goes_over(4 * group)))
+            def _():
+                out[:, block_at(zh, n)] = total
+
+    attend(2)
     attend(3)
-
-    for i in range(1, 4):
-        source = lax.rem(z + i, 4)
-        m_arrival(2 * lax.rem(source, 2) + lax.div(source, 2)).wait_recv()
-    out[...] = jnp.concatenate(
-        [m_buf[h].astype(jnp.float32) for h in range(4)], axis=1).astype(jnp.bfloat16)
-
-    for i in range(1, 4):
-        m_copy(lax.rem(z + i, 4)).wait_send()
+    project_out(0)
+    project_out(1)
+    settle(0)
+    settle(1)
+    for n in range(4):
+        done_copy(n).wait_recv()
+
+    for n in range(8):
+        near_copy(n).wait_send()
+        far_copy(n).wait_send()
+    for n in range(4):
+        done_copy(n).wait_send()
+    wm_over_z().wait_send()
+    wm_over_y().wait_send()
+    wm_relay().wait_send()
 
     @pl.loop(0, 4)
     def _(b):
-        kv_copy(b).wait_send()
+        for there in range(2):
+            @pl.when(lax.rem(b + 2 * there, 4) != z)
+            def _():
+                m_copy(b, there).wait_send()
+        for i in range(2):
+            ky_copy(i, b).wait_send()
         for i in range(3):
             c_copy(i, b).wait_send()
 
     for i in range(3):
-        w_over_z(i).wait_send()
+        if i < 2:
+            w_over_z(i).wait_send()
         w_over_y(i).wait_send()
         w_relay(i).wait_send()
 
-    @pl.when(jnp.logical_not(straight))
+    @pl.when(bent)
     def _():
         x_swap().wait_send()
 
-    @pl.when(jnp.logical_not(hub))
+    @pl.when(hub)
+    def _():
+        x_near().wait_send()
+
+    @pl.when(spoke)
     def _():
         x_cross().wait_send()
 
-    @pl.when(hub)
-    def _():
-        x_move(1, slot(x, z), at_z(z_near)).wait_send()
-
     for step in range(4):
-        b = order[step]
-
-        @pl.when(hub)
+        leads = hub if step < 2 else spoke
+
+        @pl.when(leads)
         def _():
-            x_move(2 + 2 * step, slot(x, b), (s, t_flip)).wait_send()
-            x_move(3 + 2 * step, slot(x, b), (s, t_core)).wait_send()
+            x_sideways(step).wait_send()
+            x_inside(step).wait_send()
             if step > 1:
                 @pl.when(inner)
                 def _():
-                    x_move(8 + step, slot(x, b), at_z(z_near)).wait_send()
-
-        @pl.when(jnp.logical_not(hub))
+                    x_outward(step).wait_send()
+
+        @pl.when(jnp.logical_not(leads))
         def _():
-            x_move(3 + 2 * step, slot(1 - x, b), (s, t_core)).wait_send()
-
-
-def halves(activity, wq, wk, wv):
+            x_back(step).wait_send()
+
+
+def halves(activity, wq, wk, wv, wm):
     tok, feat = activity.shape
     krows, col_width = wq.shape
     width = col_width // 4
     rows = 4 * tok
+    piece = tok // 4
+    cols = wm.shape[1]
     dma = pltpu.SemaphoreType.DMA
     return pl.pallas_call(
         halves_kernel,
-        out_shape=jax.ShapeDtypeStruct((tok, 4 * HEAD), jnp.bfloat16),
-        in_specs=[pl.BlockSpec(memory_space=pl.ANY)] * 4,
+        out_shape=jax.ShapeDtypeStruct((piece, 8 * cols), jnp.bfloat16),
+        in_specs=[pl.BlockSpec(memory_space=pltpu.HBM)] * 5,
         out_specs=pl.BlockSpec(memory_space=pltpu.VMEM),
         scratch_shapes=[
             pltpu.VMEM((9, tok, feat), jnp.bfloat16),
             pltpu.VMEM((3, 4 * krows, 2 * width), jnp.bfloat16),
-            pltpu.VMEM((3, 4, tok, width), jnp.float32),
+            pltpu.VMEM((3, 4, tok // 2, 2 * width), jnp.float32),
             pltpu.VMEM((3, 4, tok // 2, 2 * width), jnp.bfloat16),
             pltpu.VMEM((3, 4, tok // 2, 2 * width), jnp.bfloat16),
             pltpu.VMEM((rows, width), jnp.bfloat16),
             pltpu.VMEM((SPAN * DILATIONS[-1] + 2 * rows, 2 * width), jnp.bfloat16),
+            pltpu.VMEM((2, 4, tok // 2, 2 * width), jnp.bfloat16),
+            pltpu.VMEM((2, 4, tok // 2, 2 * width), jnp.bfloat16),
             pltpu.VMEM((4, tok, HEAD), jnp.bfloat16),
-            pltpu.VMEM((4, tok, HEAD), jnp.bfloat16),
-            pltpu.VMEM((rows, 128), jnp.float32),
-            pltpu.VMEM((rows, 128), jnp.float32),
+            pltpu.VMEM((2, 4, tok, HEAD), jnp.bfloat16),
+            pltpu.VMEM((4, tok // 2, 2 * width), jnp.float32),
+            pltpu.VMEM((4, tok // 2, 2 * width), jnp.float32),
+            pltpu.VMEM((4, tok, cols), jnp.bfloat16),
+            pltpu.VMEM((2, tok, 4 * HEAD), jnp.bfloat16),
+            pltpu.VMEM((8, 2, piece, cols), jnp.bfloat16),
+            pltpu.VMEM((8, 2, piece, cols), jnp.bfloat16),
+            pltpu.VMEM((8, piece, cols), jnp.bfloat16),
+            pltpu.VMEM((8, piece, cols), jnp.bfloat16),
+            pltpu.VMEM((8, 2, piece, cols), jnp.float32),
+            pltpu.VMEM((4, piece, cols), jnp.bfloat16),
             dma, dma((3,)), dma((12,)), dma((9,)), dma((3, 3)), dma((3, 3)),
-            dma((3, 4)), dma((3, 4)), dma((4,)), dma((4,)), dma((4,)), dma((4,)),
+            dma((3, 4)), dma((3, 4)), dma((2, 4)), dma((2, 4)), dma((2, 4)), dma((2, 4)),
+            dma, dma((3,)), dma((4,)), dma((8,)), dma((8,)), dma((8,)), dma((8,)),
+            dma((4,)), dma((4,)),
         ],
         compiler_params=pltpu.CompilerParams(
-            collective_id=2, has_side_effects=True, vmem_limit_bytes=58 * 2**20),
+            collective_id=2, has_side_effects=True, vmem_limit_bytes=66400000),
         cost_estimate=pl.CostEstimate(
             flops=2 * rows * feat * 3 * col_width, bytes_accessed=300 * 2**20, transcendentals=0),
-    )(activity, wq, wk, wv)
+    )(activity, wq, wk, wv, wm)
 
 
 def per_device(activity, query_weight, key_weight, value_weight, merge_weight):
@@ -807,10 +1052,9 @@
     R = lax.axis_size("sp") // G
     r = lax.axis_index("sp") % R
     tok = activity.shape[0]
+    if G == 4 and R == 2:
+        return halves(activity, query_weight, key_weight, value_weight, merge_weight)
     merge_full = lax.all_gather(merge_weight, "sp", axis=1, tiled=True)
-    if G == 4 and R == 2:
-        merged = halves(activity, query_weight, key_weight, value_weight)
-        return finish(merged, merge_full, 8)
     block_start = (jnp.arange(G, dtype=jnp.int32) * R + r) * tok
     pos = (block_start[:, None] + jnp.arange(tok, dtype=jnp.int32)[None, :]).reshape(G * tok)
     half = HEAD // 2

time: 185 us -> 125 us (0.68)
  Pallas kernels: 166 us -> 123 us
  between operations: 13.4 us -> 0.01 us
    pallas_call x2 -> x1, Pallas kernels: 166 us -> 123 us  [halves(): pl.pallas_call(halves_kernel, out_shape=jax.ShapeDtypeStruct((piece, 8 *...]
  transfers between devices with their start and end apart: 1 -> 0, of which waited for: 0 -> 0; matrix products, arithmetic and copies ran while one was open for 0% -> 0% of each run, Pallas kernels for 81% -> 0%
where the time goes in v3:
time: 125 us; the launch traced here: 124 us
  Pallas kernels  123 us (98%)
  local copies, waits for them, and re-layouts  1.87 us (1%)
    pallas_call x1, Pallas kernels, halves(): pl.pallas_call(halves_kernel, out_shape=jax.ShapeDtypeStruct((piece, 8 *...  123 us

profile of v3, /device:TPU:25, one launch (start us, length us, event | category | flops | bytes accessed | tf_op | source)
XLA Modules:
  0.0 124.4 jit_solution(8874407293320254523)
XLA Ops:
  0.0 122.5 %shard_map.55 = bf16[64,4096]{1,0:T(8,128)(2,1)} custom-call(bf16[256,1024]{1,0:T(8,128)(2,1)} %act.1, bf16[512,768]{1,0:T(8,128)(2,1)} %wq.1, bf16[512,768]{1,0:T(8,128)(2,1)} %wk.1, bf16[512,768]{1,0:T(8,128)(2,1)} %wv.1, bf16[256,512]{1,0:T(8,128)(2,1)} %wm.1), custom_call_target="tpu_custom_call" | custom-call | flops 4831838208 | bytes 314572800 | tf_op jit(solution)/shard_map/pallas_call | solution.py:1011
  122.5 1.9 %copy.7 = bf16[64,4096]{1,0:T(8,128)(2,1)} copy(bf16[64,4096]{1,0:T(8,128)(2,1)} %shard_map.55) | data formatting | bytes 1048576

commit v4 on v3

--- a/solution.py
+++ b/solution.py
@@ -412,7 +412,7 @@
     act, wq, wk, wv, wm, out,
     x_buf, w_buf, own_buf, c_buf, r_buf, q_buf, kv_buf, ky_out, ky_in, o_buf, m_buf,
     cos_buf, sin_buf, wm_buf, merged_buf, near_out, near_in, far_out, far_in, held,
-    done_out,
+    done_out, prob_buf, gain_buf,
     local_sem, w_local, x_send, x_recv, w_send, w_recv, c_send, c_recv,
     ky_send, ky_recv, m_send, m_recv, wm_local, wm_send, wm_recv,
     near_send, near_recv, far_send, far_recv, done_send, done_recv,
@@ -430,7 +430,7 @@
     pair = wq.shape[1] // 2
     width = pair // 2
     part = tok // 2
-    weights = (wk, wq, wv)
+    weights = (wk, wv, wq)
     z_near = z + 1 - 2 * zl
     z_pair = lax.rem(z + 2, 4)
     y_far = 1 - y
@@ -565,7 +565,8 @@
             @pl.when(inner)
             def _():
                 x_outward(step).start()
-        x_sideways(step).start()
+        if step > 0:
+            x_sideways(step).start()
         x_inside(step).start()
 
     def follow(step):
@@ -617,7 +618,6 @@
             x_near().start()
             lead(0)
             w_over_z(1).start()
-            w_over_z(2).start()
 
         @pl.when(spoke)
         def _():
@@ -651,6 +651,10 @@
     w_relay(0).start()
     w_over_y(1).start()
 
+    @pl.when(hub)
+    def _():
+        x_sideways(0).start()
+
     @pl.when(spoke)
     def _():
         follow(0)
@@ -667,17 +671,17 @@
     other_arrived(0)
     part_sum(0, order[0], False)
 
+    @pl.when(spoke & inner)
+    def _():
+        lead(3)
+
     w_over_z(1).wait_recv()
     w_relay(1).start()
     w_over_y(2).start()
+    w_over_z(2).start()
 
     @pl.when(spoke)
     def _():
-        @pl.when(inner)
-        def _():
-            lead(3)
-
-        w_over_z(2).start()
         follow(1)
 
     @pl.when(hub & inner)
@@ -710,7 +714,7 @@
     w_over_z(2).wait_recv()
     w_relay(2).start()
     other_arrived(2)
-    part_sum(0, order[2], True)
+    part_sum(0, order[2], False)
     part_sum(1, order[2], True)
 
     @pl.when(hub & outer)
@@ -718,19 +722,16 @@
         follow(3)
 
     other_arrived(3)
-    part_sum(0, order[3], True)
+    part_sum(0, order[3], False)
     part_sum(1, order[3], True)
 
     w_over_z(2).wait_send()
     wm_over_z().start()
-    wm_over_y().start()
 
     @pl.when(inner)
     def _():
-        for i in range(2):
-            for step in range(4):
-                if i == 1 or step > 1:
-                    c_copy(i, order[step]).start()
+        for b in range(2):
+            c_copy(1, b).start()
 
     most = SPAN * DILATIONS[-1]
     kv_buf[0:most, :] = jnp.zeros((most, 2 * width), jnp.bfloat16)
@@ -739,6 +740,10 @@
 
     @pl.loop(0, 4)
     def _(b):
+        @pl.when(inner & (b > 0) & (b < 3))
+        def _():
+            c_copy(1, b + 1).start()
+
         part_sum(2, b, False)
 
     def kv_rows(b, which):
@@ -771,23 +776,22 @@
         ky_copy(0, b).start()
         kv_buf[kv_rows(b, y), :width] = unpacked(turned)
 
-    wm_came(wm_near_slot)
-    wm_relay().start()
-
-    for step in range(4):
-        b = theirs[step]
-        rows = pl.ds(pl.multiple_of(b * tok, tok), tok)
-        q_buf[rows, :] = unpacked(rotate(whole_sum(1, b), b))
 
     def gather_values(b):
-        value = whole_sum(2, b).astype(jnp.bfloat16)
+        value = whole_sum(1, b).astype(jnp.bfloat16)
         ky_out[1, b] = value
         ky_copy(1, b).start()
         kv_buf[kv_rows(b, y), width:] = unpacked(value)
 
-    def values_arrived(b):
+    def gather_queries(b):
+        rows = pl.ds(pl.multiple_of(b * tok, tok), tok)
+        q_buf[rows, :] = unpacked(rotate(whole_sum(2, b), b))
+
+    def keys_arrived(b):
         ky_copy(0, b).wait_recv()
         kv_buf[kv_rows(b, y_far), :width] = unpacked(ky_in[0, b])
+
+    def values_arrived(b):
         ky_copy(1, b).wait_recv()
         kv_buf[kv_rows(b, y_far), width:] = unpacked(ky_in[1, b])
 
@@ -802,19 +806,23 @@
         return remote(m_buf.at[there, source], m_buf.at[there, source], m_send.at[there, source],
                       m_recv.at[there, source], at_z(z))
 
-    def attend(b):
-        values_arrived(b)
+    spans = [SPAN * dilation + tok for dilation in DILATIONS]
+    places = [sum(spans[:index]) for index in range(HEAD_GROUPS)]
+
+    def near_keys(index, b):
+        first = (b * 2 + y) * tok
+        return pl.ds(pl.multiple_of(most - SPAN * DILATIONS[index] + first, 128), spans[index])
+
+    def weigh(b):
         rows = pl.ds(pl.multiple_of(b * tok, tok), tok)
         first = (b * 2 + y) * tok
-        mixed_list = []
+        sum_list = []
         total_list = []
         for index, dilation in enumerate(DILATIONS):
             reach = SPAN * dilation
-            keys = reach + tok
-            near = pl.ds(pl.multiple_of(most - reach + first, 128), keys)
+            keys = spans[index]
             q = q_buf[rows, index * HEAD:(index + 1) * HEAD]
-            k = kv_buf[near, index * HEAD:(index + 1) * HEAD]
-            v = kv_buf[near, width + index * HEAD:width + (index + 1) * HEAD]
+            k = kv_buf[near_keys(index, b), index * HEAD:(index + 1) * HEAD]
             scores = lax.dot_general(
                 q, k, (((1,), (1,)), ((), ())), preferred_element_type=jnp.float32
             ) * HEAD ** (-0.5)
@@ -827,13 +835,23 @@
             row_max = jnp.max(scores, axis=1, keepdims=True)
             expo = jnp.exp(scores - row_max)
             denominator = jnp.sum(expo, axis=1, keepdims=True)
-            mixed = jnp.dot(expo.astype(jnp.bfloat16), v, preferred_element_type=jnp.float32)
-            mixed_list.append(mixed / denominator)
+            prob_buf[b, :, places[index]:places[index] + keys] = expo.astype(jnp.bfloat16)
+            sum_list.append(denominator)
             total_list.append(row_max + jnp.log(denominator))
         peak = jnp.maximum(jnp.maximum(total_list[0], total_list[1]), total_list[2])
         shifted = [jnp.exp(one - peak) for one in total_list]
         whole = shifted[0] + shifted[1] + shifted[2]
-        merged = sum(a / whole * b_ for a, b_ in zip(shifted, mixed_list)).astype(jnp.bfloat16)
+        for index in range(HEAD_GROUPS):
+            gain_buf[b, index] = shifted[index] / whole / sum_list[index]
+
+    def attend(b):
+        merged = jnp.zeros((tok, HEAD), jnp.float32)
+        for index in range(HEAD_GROUPS):
+            v = kv_buf[near_keys(index, b), width + index * HEAD:width + (index + 1) * HEAD]
+            prob = prob_buf[b, :, places[index]:places[index] + spans[index]]
+            mixed = jnp.dot(prob, v, preferred_element_type=jnp.float32)
+            merged = merged + gain_buf[b, index] * mixed
+        merged = packed(merged).astype(jnp.bfloat16)
         o_buf[b] = merged
         for there in range(2):
             mine = lax.rem(b + 2 * there, 4) == z
@@ -845,17 +863,6 @@
             @pl.when(mine)
             def _():
                 m_buf[there, head] = merged
-
-    gather_values(0)
-
-    gather_values(1)
-
-    @pl.loop(2, 4)
-    def _(b):
-        gather_values(b)
-        attend(b - 2)
-
-    wm_here().wait()
 
     far = lax.rem(t + 2, 4)
     across = 3 - t
@@ -870,11 +877,8 @@
 
     blocks = (wm_slot, wm_near_slot, zl * 2 + y_far, (1 - zl) * 2 + y_far)
 
-    def goes_over(n):
-        return zh == 1 - n // 4
-
     def product(n):
-        there = zh if n < 4 else 1 - zh
+        there = 1 - n // 4
         block = blocks[n % 4]
 
         def rows_of(owner):
@@ -904,44 +908,68 @@
                       done_recv.at[n], at_z(z_pair))
 
     def collect(group):
-        there = zh if group == 0 else 1 - zh
+        there = 1 - group
         for i in range(1, 4):
             source = lax.rem(z + i, 4)
             m_arrival(there, 2 * lax.rem(source, 2) + lax.div(source, 2)).wait_recv()
-        merged_buf[there] = jnp.concatenate(
-            [m_buf[there, h].astype(jnp.float32) for h in range(4)], axis=1).astype(jnp.bfloat16)
-
-    def project_out(group):
-        collect(group)
-        for n in range(4 * group, 4 * group + 4):
-            if n == 2:
-                wm_came(blocks[2])
-            if n == 3:
-                wm_came(blocks[3])
-            product(n)
-            if n > 4 * group:
-                pass_on(n - 1)
-        pass_on(4 * group + 3)
-
-    def settle(group):
-        for n in range(4):
-            total = total_of(4 * group + n)
-
-            @pl.when(goes_over(4 * group))
-            def _():
-                done_out[n] = total
-                done_copy(n).start()
-
-            @pl.when(jnp.logical_not(goes_over(4 * group)))
-            def _():
-                out[:, block_at(zh, n)] = total
-
-    attend(2)
-    attend(3)
-    project_out(0)
-    project_out(1)
-    settle(0)
-    settle(1)
+        heads = [m_buf[there, h].astype(jnp.float32) for h in range(4)]
+        for half in range(2):
+            merged_buf[there, half * part:(half + 1) * part] = jnp.concatenate(
+                [one[:, half * HEAD:(half + 1) * HEAD] for one in heads], axis=1).astype(jnp.bfloat16)
+
+    def hand_over(n):
+        done_out[n] = total_of(n)
+        done_copy(n).start()
+
+    def finish_block(b):
+        gather_queries(b)
+        keys_arrived(b)
+        values_arrived(b)
+        weigh(b)
+        attend(b)
+
+    wm_over_y().start()
+    gather_values(0)
+    gather_values(1)
+
+    @pl.when(inner)
+    def _():
+        gather_values(2)
+        gather_values(3)
+
+    wm_here().wait()
+    wm_came(wm_near_slot)
+    wm_relay().start()
+
+    for b in range(2):
+        finish_block(b)
+
+        @pl.when(outer)
+        def _():
+            gather_values(b + 2)
+
+    finish_block(2)
+    finish_block(3)
+    collect(0)
+    for n in range(4):
+        if n == 2:
+            wm_came(blocks[2])
+        if n == 3:
+            wm_came(blocks[3])
+        product(n)
+        if n > 0:
+            pass_on(n - 1)
+    pass_on(3)
+    hand_over(0)
+    collect(1)
+    for n in range(4, 8):
+        product(n)
+        if n > 4:
+            pass_on(n - 1)
+            hand_over(n - 4)
+    pass_on(7)
+    for n in range(4, 8):
+        out[:, block_at(zh, n - 4)] = total_of(n)
     for n in range(4):
         done_copy(n).wait_recv()
 
@@ -1023,8 +1051,8 @@
             pltpu.VMEM((SPAN * DILATIONS[-1] + 2 * rows, 2 * width), jnp.bfloat16),
             pltpu.VMEM((2, 4, tok // 2, 2 * width), jnp.bfloat16),
             pltpu.VMEM((2, 4, tok // 2, 2 * width), jnp.bfloat16),
-            pltpu.VMEM((4, tok, HEAD), jnp.bfloat16),
-            pltpu.VMEM((2, 4, tok, HEAD), jnp.bfloat16),
+            pltpu.VMEM((4, tok // 2, 2 * HEAD), jnp.bfloat16),
+            pltpu.VMEM((2, 4, tok // 2, 2 * HEAD), jnp.bfloat16),
             pltpu.VMEM((4, tok // 2, 2 * width), jnp.float32),
             pltpu.VMEM((4, tok // 2, 2 * width), jnp.float32),
             pltpu.VMEM((4, tok, cols), jnp.bfloat16),
@@ -1035,6 +1063,8 @@
             pltpu.VMEM((8, piece, cols), jnp.bfloat16),
             pltpu.VMEM((8, 2, piece, cols), jnp.float32),
             pltpu.VMEM((4, piece, cols), jnp.bfloat16),
+            pltpu.VMEM((4, tok, sum(SPAN * one + tok for one in DILATIONS)), jnp.bfloat16),
+            pltpu.VMEM((4, HEAD_GROUPS, tok, 1), jnp.float32),
             dma, dma((3,)), dma((12,)), dma((9,)), dma((3, 3)), dma((3, 3)),
             dma((3, 4)), dma((3, 4)), dma((2, 4)), dma((2, 4)), dma((2, 4)), dma((2, 4)),
             dma, dma((3,)), dma((4,)), dma((8,)), dma((8,)), dma((8,)), dma((8,)),

time: 125 us -> 119 us (0.952)
  Pallas kernels: 123 us -> 115 us
    pallas_call x1, Pallas kernels: 123 us -> 115 us  [halves(): pl.pallas_call(halves_kernel, out_shape=jax.ShapeDtypeStruct((piece, 8 *...]
where the time goes in v4:
time: 119 us; the launch traced here: 117 us
  Pallas kernels  115 us (97%)
  local copies, waits for them, and re-layouts  1.87 us (2%)
    pallas_call x1, Pallas kernels, halves(): pl.pallas_call(halves_kernel, out_shape=jax.ShapeDtypeStruct((piece, 8 *...  115 us

profile of v4, /device:TPU:25, one launch (start us, length us, event | category | flops | bytes accessed | tf_op | source)
XLA Modules:
  0.0 117.3 jit_solution(8144501857761923154)
XLA Ops:
  0.0 115.5 %shard_map.55 = bf16[64,4096]{1,0:T(8,128)(2,1)} custom-call(bf16[256,1024]{1,0:T(8,128)(2,1)} %act.1, bf16[512,768]{1,0:T(8,128)(2,1)} %wq.1, bf16[512,768]{1,0:T(8,128)(2,1)} %wk.1, bf16[512,768]{1,0:T(8,128)(2,1)} %wv.1, bf16[256,512]{1,0:T(8,128)(2,1)} %wm.1), custom_call_target="tpu_custom_call" | custom-call | flops 4831838208 | bytes 314572800 | tf_op jit(solution)/shard_map/pallas_call | solution.py:1039
  115.5 1.9 %copy.7 = bf16[64,4096]{1,0:T(8,128)(2,1)} copy(bf16[64,4096]{1,0:T(8,128)(2,1)} %shard_map.55) | data formatting | bytes 1048576

commit v5 on v4

--- a/solution.py
+++ b/solution.py
@@ -409,13 +409,13 @@
 
 
 def halves_kernel(
-    act, wq, wk, wv, wm, out,
+    act, wq, wk, wv, wm, out_hbm,
     x_buf, w_buf, own_buf, c_buf, r_buf, q_buf, kv_buf, ky_out, ky_in, o_buf, m_buf,
     cos_buf, sin_buf, wm_buf, merged_buf, near_out, near_in, far_out, far_in, held,
-    done_out, prob_buf, gain_buf,
+    done_out, prob_buf, gain_buf, out,
     local_sem, w_local, x_send, x_recv, w_send, w_recv, c_send, c_recv,
     ky_send, ky_recv, m_send, m_recv, wm_local, wm_send, wm_recv,
-    near_send, near_recv, far_send, far_recv, done_send, done_recv,
+    near_send, near_recv, far_send, far_recv, done_send, done_recv, out_sem,
 ):
     s = lax.axis_index("sp")
     t = lax.axis_index("tp")
@@ -475,28 +475,44 @@
         return pl.ds(pl.multiple_of(p * pair, 128), pair)
 
     mine_rows = own_rows(zl * 2 + y)
-    near_rows = own_rows((1 - zl) * 2 + y)
 
     def w_own(i):
         return pltpu.make_async_copy(
             weights[i].at[:, pair_cols(zl)], w_buf.at[i, mine_rows], w_local.at[i])
 
-    def w_over_z(i):
-        return remote(weights[i].at[:, pair_cols(1 - zl)], w_buf.at[i, mine_rows],
-                      w_send.at[0, i], w_recv.at[0, i], at_z(z_near))
+    small = krows // 2
+
+    def piece_rows(block, p):
+        return pl.ds(pl.multiple_of(block * krows + p * small, 128), small)
+
+    def w_over_z(i, p):
+        return remote(weights[i].at[p * small:(p + 1) * small, pair_cols(1 - zl)],
+                      w_buf.at[i, piece_rows(zl * 2 + y, p)],
+                      w_send.at[p, i], w_recv.at[p, i], at_z(z_near))
 
     def w_over_y(i):
         return remote(weights[i].at[:, pair_cols(zl)], w_buf.at[i, mine_rows],
-                      w_send.at[1, i], w_recv.at[1, i], y_dev)
-
-    def w_relay(i):
-        return remote(w_buf.at[i, near_rows], w_buf.at[i, near_rows],
-                      w_send.at[2, i], w_recv.at[2, i], y_dev)
+                      w_send.at[4, i], w_recv.at[4, i], y_dev)
+
+    def w_relay(i, p):
+        rows = piece_rows((1 - zl) * 2 + y, p)
+        return remote(w_buf.at[i, rows], w_buf.at[i, rows],
+                      w_send.at[2 + p, i], w_recv.at[2 + p, i], y_dev)
+
+    def w_push(i):
+        for p in range(2):
+            w_over_z(i, p).start()
+
+    def w_hand_on(i):
+        for p in range(2):
+            w_over_z(i, p).wait_recv()
+            w_relay(i, p).start()
 
     def w_wait(i):
         w_own(i).wait()
         w_over_y(i).wait_recv()
-        w_relay(i).wait_recv()
+        w_relay(i, 0).wait_recv()
+        w_relay(i, 1).wait_recv()
 
     wm_slot = zl * 2 + y
     wm_near_slot = (1 - zl) * 2 + y
@@ -597,7 +613,7 @@
             def _():
                 c_copy(i, b).start()
 
-    w_over_z(0).start()
+    w_push(0)
     w_over_y(0).start()
 
     @pl.when(bent)
@@ -617,12 +633,12 @@
         def _():
             x_near().start()
             lead(0)
-            w_over_z(1).start()
+            w_push(1)
 
         @pl.when(spoke)
         def _():
             x_cross().start()
-            w_over_z(1).start()
+            w_push(1)
 
     @pl.when(straight)
     def _():
@@ -647,8 +663,7 @@
         x_arrived(x_here())
         x_first()
 
-    w_over_z(0).wait_recv()
-    w_relay(0).start()
+    w_hand_on(0)
     w_over_y(1).start()
 
     @pl.when(hub)
@@ -675,10 +690,9 @@
     def _():
         lead(3)
 
-    w_over_z(1).wait_recv()
-    w_relay(1).start()
+    w_hand_on(1)
     w_over_y(2).start()
-    w_over_z(2).start()
+    w_push(2)
 
     @pl.when(spoke)
     def _():
@@ -711,8 +725,7 @@
     def _():
         follow(2)
 
-    w_over_z(2).wait_recv()
-    w_relay(2).start()
+    w_hand_on(2)
     other_arrived(2)
     part_sum(0, order[2], False)
     part_sum(1, order[2], True)
@@ -725,7 +738,8 @@
     part_sum(0, order[3], False)
     part_sum(1, order[3], True)
 
-    w_over_z(2).wait_send()
+    for p in range(2):
+        w_over_z(2, p).wait_send()
     wm_over_z().start()
 
     @pl.when(inner)
@@ -739,12 +753,12 @@
     w_wait(2)
 
     @pl.loop(0, 4)
-    def _(b):
-        @pl.when(inner & (b > 0) & (b < 3))
+    def _(n):
+        @pl.when(inner & (n > 0) & (n < 3))
         def _():
-            c_copy(1, b + 1).start()
-
-        part_sum(2, b, False)
+            c_copy(1, n + 1).start()
+
+        part_sum(2, jnp.where(n == 3, 3, lax.rem(2 * n, 3)), False)
 
     def kv_rows(b, which):
         return pl.ds(pl.multiple_of(most + (b * 2 + which) * tok, 128), tok)
@@ -903,6 +917,10 @@
     def block_at(half, n):
         return pl.ds(pl.multiple_of((half * 4 + blocks[n]) * cols, 128), cols)
 
+    def out_copy(half, n):
+        at = block_at(half, n)
+        return pltpu.make_async_copy(out.at[:, at], out_hbm.at[:, at], out_sem.at[half, n])
+
     def done_copy(n):
         return remote(done_out.at[n], out.at[:, block_at(zh, n)], done_send.at[n],
                       done_recv.at[n], at_z(z_pair))
@@ -918,13 +936,19 @@
                 [one[:, half * HEAD:(half + 1) * HEAD] for one in heads], axis=1).astype(jnp.bfloat16)
 
     def hand_over(n):
-        done_out[n] = total_of(n)
-        done_copy(n).start()
-
-    def finish_block(b):
+        total = total_of(n)
+        if n < 4:
+            done_out[n] = total
+            done_copy(n).start()
+        else:
+            out[:, block_at(zh, n - 4)] = total
+            out_copy(zh, n - 4).start()
+
+    def finish_block(b, fresh):
         gather_queries(b)
-        keys_arrived(b)
-        values_arrived(b)
+        for one in fresh:
+            keys_arrived(one)
+            values_arrived(one)
         weigh(b)
         attend(b)
 
@@ -941,15 +965,20 @@
     wm_came(wm_near_slot)
     wm_relay().start()
 
-    for b in range(2):
-        finish_block(b)
-
-        @pl.when(outer)
-        def _():
-            gather_values(b + 2)
-
-    finish_block(2)
-    finish_block(3)
+    finish_block(0, (0,))
+
+    @pl.when(outer)
+    def _():
+        gather_values(2)
+
+    finish_block(2, (1, 2))
+
+    @pl.when(outer)
+    def _():
+        gather_values(3)
+
+    finish_block(1, ())
+    finish_block(3, (3,))
     collect(0)
     for n in range(4):
         if n == 2:
@@ -969,9 +998,13 @@
             hand_over(n - 4)
     pass_on(7)
     for n in range(4, 8):
-        out[:, block_at(zh, n - 4)] = total_of(n)
+        hand_over(n)
     for n in range(4):
         done_copy(n).wait_recv()
+        out_copy(1 - zh, n).start()
+    for n in range(4):
+        out_copy(zh, n).wait()
+        out_copy(1 - zh, n).wait()
 
     for n in range(8):
         near_copy(n).wait_send()
@@ -994,10 +1027,11 @@
             c_copy(i, b).wait_send()
 
     for i in range(3):
-        if i < 2:
-            w_over_z(i).wait_send()
+        for p in range(2):
+            if i < 2:
+                w_over_z(i, p).wait_send()
+            w_relay(i, p).wait_send()
         w_over_y(i).wait_send()
-        w_relay(i).wait_send()
 
     @pl.when(bent)
     def _():
@@ -1040,7 +1074,7 @@
         halves_kernel,
         out_shape=jax.ShapeDtypeStruct((piece, 8 * cols), jnp.bfloat16),
         in_specs=[pl.BlockSpec(memory_space=pltpu.HBM)] * 5,
-        out_specs=pl.BlockSpec(memory_space=pltpu.VMEM),
+        out_specs=pl.BlockSpec(memory_space=pltpu.HBM),
         scratch_shapes=[
             pltpu.VMEM((9, tok, feat), jnp.bfloat16),
             pltpu.VMEM((3, 4 * krows, 2 * width), jnp.bfloat16),
@@ -1065,10 +1099,11 @@
             pltpu.VMEM((4, piece, cols), jnp.bfloat16),
             pltpu.VMEM((4, tok, sum(SPAN * one + tok for one in DILATIONS)), jnp.bfloat16),
             pltpu.VMEM((4, HEAD_GROUPS, tok, 1), jnp.float32),
-            dma, dma((3,)), dma((12,)), dma((9,)), dma((3, 3)), dma((3, 3)),
+            pltpu.VMEM((piece, 8 * cols), jnp.bfloat16),
+            dma, dma((3,)), dma((12,)), dma((9,)), dma((5, 3)), dma((5, 3)),
             dma((3, 4)), dma((3, 4)), dma((2, 4)), dma((2, 4)), dma((2, 4)), dma((2, 4)),
             dma, dma((3,)), dma((4,)), dma((8,)), dma((8,)), dma((8,)), dma((8,)),
-            dma((4,)), dma((4,)),
+            dma((4,)), dma((4,)), dma((2, 4)),
         ],
         compiler_params=pltpu.CompilerParams(
             collective_id=2, has_side_effects=True, vmem_limit_bytes=66400000),

time: 119 us -> 117 us (0.983); the launches traced: 117 us -> 117 us
  no operation moved by 1% of the time
where the time goes in v5:
time: 117 us
  Pallas kernels  115 us (98%)
  local copies, waits for them, and re-layouts  1.87 us (2%)
    pallas_call x1, Pallas kernels, halves(): pl.pallas_call(halves_kernel, out_shape=jax.ShapeDtypeStruct((piece, 8 *...  115 us

profile of v5, /device:TPU:25, one launch (start us, length us, event | category | flops | bytes accessed | tf_op | source)
XLA Modules:
  0.0 116.9 jit_solution(1903294450475362671)
XLA Ops:
  0.0 115.0 %shard_map.55 = bf16[64,4096]{1,0:T(8,128)(2,1)} custom-call(bf16[256,1024]{1,0:T(8,128)(2,1)} %act.1, bf16[512,768]{1,0:T(8,128)(2,1)} %wq.1, bf16[512,768]{1,0:T(8,128)(2,1)} %wk.1, bf16[512,768]{1,0:T(8,128)(2,1)} %wv.1, bf16[256,512]{1,0:T(8,128)(2,1)} %wm.1), custom_call_target="tpu_custom_call" | custom-call | flops 4831838208 | bytes 314572800 | tf_op jit(solution)/shard_map/pallas_call | solution.py:1073
  115.0 1.9 %copy.7 = bf16[64,4096]{1,0:T(8,128)(2,1)} copy(bf16[64,4096]{1,0:T(8,128)(2,1)} %shard_map.55) | data formatting | bytes 1048576

commit v6 on v5

--- a/solution.py
+++ b/solution.py
@@ -741,6 +741,7 @@
     for p in range(2):
         w_over_z(2, p).wait_send()
     wm_over_z().start()
+    wm_over_y().start()
 
     @pl.when(inner)
     def _():
@@ -952,7 +953,6 @@
         weigh(b)
         attend(b)
 
-    wm_over_y().start()
     gather_values(0)
     gather_values(1)
 

time: 117 us -> 117 us (level); the launches traced: 117 us -> 116 us
    pallas_call x1, Pallas kernels: 115 us -> 114 us  [halves(): pl.pallas_call(halves_kernel, out_shape=jax.ShapeDtypeStruct((piece, 8 *...]
where the time goes in v6:
time: 117 us; the launch traced here: 116 us
  Pallas kernels  114 us (97%)
  local copies, waits for them, and re-layouts  1.87 us (2%)
    pallas_call x1, Pallas kernels, halves(): pl.pallas_call(halves_kernel, out_shape=jax.ShapeDtypeStruct((piece, 8 *...  114 us

profile of v6, /device:TPU:25, one launch (start us, length us, event | category | flops | bytes accessed | tf_op | source)
XLA Modules:
  0.0 115.7 jit_solution(14223071574016233616)
XLA Ops:
  0.0 113.8 %shard_map.55 = bf16[64,4096]{1,0:T(8,128)(2,1)} custom-call(bf16[256,1024]{1,0:T(8,128)(2,1)} %act.1, bf16[512,768]{1,0:T(8,128)(2,1)} %wq.1, bf16[512,768]{1,0:T(8,128)(2,1)} %wk.1, bf16[512,768]{1,0:T(8,128)(2,1)} %wv.1, bf16[256,512]{1,0:T(8,128)(2,1)} %wm.1), custom_call_target="tpu_custom_call" | custom-call | flops 4831838208 | bytes 314572800 | tf_op jit(solution)/shard_map/pallas_call | solution.py:1073
  113.8 1.9 %copy.7 = bf16[64,4096]{1,0:T(8,128)(2,1)} copy(bf16[64,4096]{1,0:T(8,128)(2,1)} %shard_map.55) | data formatting | bytes 1048576
